TPU v7x, 128 devices: a whole 4x4x4 slice. The times are simulated.
128 devices in a mesh: ep: 32 (over z, y, core), tp: 4 (over x).
Axes of the slice: x: 4, y: 4, z: 4, core: 2. Of those that a mesh axis runs over, the one named last changes fastest.
Arguments:
- tokens: bfloat16 [512, 2048], P('ep'), may hold values from -60 to 60
- mixer_gain: float32 [2048], replicated, may hold values from 0.1 to 1.9
- query_weight: bfloat16 [2048, 2048], P('ep', 'tp'), may hold values from -0.125 to 0.125
- key_weight: bfloat16 [2048, 2048], P('ep', 'tp'), may hold values from -0.125 to 0.125
- value_weight: bfloat16 [2048, 2048], P('ep', 'tp'), may hold values from -0.125 to 0.125
- outgate_weight: bfloat16 [2048, 2048], P('ep', 'tp'), may hold values from -0.125 to 0.125
- igate_weight: bfloat16 [4, 2048], P('tp'), may hold values from -0.125 to 0.125
- fgate_weight: bfloat16 [4, 2048], P('tp'), may hold values from -0.125 to 0.125
- memory: float32 [512, 4, 512, 512], P('ep', 'tp'), may hold values from -6 to 6
- stabilizer: float32 [512, 4], P('ep', 'tp'), may hold values from -6 to 6
- head_gain: float32 [2048], P('tp'), may hold values from 0.1 to 1.9
- down_weight: bfloat16 [2048, 2048], P(None, 'ep'), may hold values from -1 to 1
- mixed_gain: float32 [2048], P('ep'), may hold values from 0.1 to 1.9
- expert_gain: float32 [2048], P('ep'), may hold values from 0.1 to 1.9
- routes: int32 [512, 4], replicated, may hold values from 0 to 31, all different within a row; in each aligned block of 16 rows (0 to 15, 16 to 31, ...) at most 4 rows name the same one
- route_weights: float32 [512, 4], replicated, may hold values from 0.1 to 1
- gate_proj: bfloat16 [32, 2048, 2048], P('ep', None, 'tp'), may hold values from -0.5 to 0.5
- up_proj: bfloat16 [32, 2048, 2048], P('ep', None, 'tp'), may hold values from -0.5 to 0.5
- expert_down: bfloat16 [32, 2048, 2048], P('ep', 'tp'), may hold values from -1 to 1
- output_gain: float32 [2048], P('tp'), may hold values from 0.1 to 1.9
Outputs:
- layer_out: bfloat16 [512, 2048], P('ep', 'tp')
Inputs may be any that keep to these rules, and one draw needn't show every extreme that they name: `routes`: each row names 4 different experts; within the rows of one device (16 rows) no expert is named more than 4 times, a bound that some block reaches.
All inputs are finite; a program needn't handle non-finite values.
Results may differ from a plain program's by a relative error of at most 0.0095.
Values may be sent and summed in bfloat16 or wider, within the bound.
A program may use at most 128 MiB of HBM per device.

v0:
```python
import jax
import jax.numpy as jnp
from jax import lax
from jax.sharding import PartitionSpec as P

NORM_EPS = 1e-06
CLAMP_LIMIT = 7.0
SIGMOID_SCALE = 1.702


def in_one_piece(arrays, axis, dim, along):
    ends, at = ([], 0)
    for a in arrays[:-1]:
        at += a.shape[along]
        ends.append(at)
    both = jnp.concatenate(arrays, axis=along)
    return tuple(jnp.split(lax.all_gather(both, axis, axis=dim, tiled=True), ends, axis=along))


def joined_along(parts, dim):
    parts = jnp.moveaxis(parts, 0, dim)
    shape = parts.shape
    return parts.reshape(*shape[:dim], shape[dim] * shape[dim + 1], *shape[dim + 2 :])


def copy_for_each(shard, axis):
    devices = lax.axis_size(axis)
    return lax.all_to_all(
        jnp.broadcast_to(shard[None], (devices, *shard.shape)), axis, 0, 0, tiled=True
    )


def gathered_copies(shard, axis, dim):
    return joined_along(copy_for_each(shard, axis), dim)


def taken_together(shard, axis):
    return copy_for_each(shard, axis).sum(axis=0)


def packed_total(arrays, axis):
    ends = [0]
    for a in arrays:
        ends.append(ends[-1] + a.size)
    subtotal = taken_together(jnp.concatenate([a.ravel() for a in arrays]), axis)
    return tuple((subtotal[b:e].reshape(a.shape) for a, b, e in zip(arrays, ends, ends[1:])))


def cut_along(shard, dim, devices):
    shape = shard.shape
    parts = shard.reshape(*shape[:dim], devices, shape[dim] // devices, *shape[dim + 1 :])
    return jnp.moveaxis(parts, dim, 0)


def sent_and_summed(shard, axis, dim):
    devices = lax.axis_size(axis)
    parts = lax.all_to_all(cut_along(shard, dim, devices), axis, 0, 0, tiled=True)
    return jnp.sum(parts.astype(jnp.float32), axis=0)


def rms_scale(values):
    return lax.rsqrt(jnp.mean(values * values, axis=-1, keepdims=True) + NORM_EPS)


def slot_tables(routes, groups, experts, capacity):
    token_total, top_count = routes.shape
    per_group = token_total // groups
    flat_routes = routes.reshape(groups, per_group * top_count)
    onehot = (
        flat_routes[:, :, None] == jnp.arange(experts, dtype=jnp.int32)[None, None, :]
    ).astype(jnp.int32)
    before = jnp.cumsum(onehot, axis=1) - onehot
    slot_index = jnp.sum(before * onehot, axis=2)
    group_ids = jnp.arange(groups, dtype=jnp.int32)[:, None]
    destination = ((flat_routes * groups + group_ids) * capacity + slot_index).reshape(
        token_total, top_count
    )
    owner_token = jnp.arange(token_total * top_count, dtype=jnp.int32) // top_count
    slot_token = (
        jnp.full((experts * groups * capacity,), token_total, jnp.int32)
        .at[destination.reshape(-1)]
        .set(owner_token)
    )
    return (destination, slot_token)


def read_memory(projected, log_input, log_forget, memory, stabilizer, head_gain):
    row_total, head_count, head_size = (memory.shape[0], memory.shape[1], memory.shape[3])
    query_scaled = projected[:, 0] * head_size ** (-0.5)
    key_rows = projected[:, 1]
    value_rows = projected[:, 2]
    outgate_rows = projected[:, 3]
    peak_log = jnp.maximum(log_forget + stabilizer, log_input)
    within = jnp.exp(log_input - peak_log)
    carried = jnp.exp(log_forget + stabilizer - peak_log)
    scores = jnp.sum(query_scaled * key_rows, axis=-1) * within
    state_read = jnp.einsum("nhd,nhde->nhe", query_scaled, memory)
    read_value = scores[..., None] * value_rows + carried[..., None] * state_read
    head_mean = jnp.mean(read_value, axis=-1, keepdims=True)
    centered = read_value - head_mean
    head_var = jnp.mean(centered * centered, axis=-1, keepdims=True)
    normalized = centered * lax.rsqrt(head_var + NORM_EPS)
    gained = normalized * head_gain.reshape(head_count, head_size) * jax.nn.sigmoid(outgate_rows)
    return gained.reshape(row_total, head_count * head_size).astype(jnp.bfloat16)


def run_experts(row_block, gate_proj, up_proj, expert_down):
    gate_pre = jnp.minimum(
        jnp.einsum("erd,edh->erh", row_block, gate_proj, preferred_element_type=jnp.float32),
        CLAMP_LIMIT,
    )
    up_pre = jnp.clip(
        jnp.einsum("erd,edh->erh", row_block, up_proj, preferred_element_type=jnp.float32),
        -CLAMP_LIMIT,
        CLAMP_LIMIT,
    )
    activation = ((up_pre + 1.0) * gate_pre * jax.nn.sigmoid(SIGMOID_SCALE * gate_pre)).astype(
        jnp.bfloat16
    )
    return jnp.einsum("erh,ehd->erd", activation, expert_down, preferred_element_type=jnp.float32)


def shards(
    tokens,
    mixer_gain,
    query_weight,
    key_weight,
    value_weight,
    outgate_weight,
    igate_weight,
    fgate_weight,
    memory,
    stabilizer,
    head_gain,
    down_weight,
    mixed_gain,
    expert_gain,
    routes,
    route_weights,
    gate_proj,
    up_proj,
    expert_down,
    output_gain,
):
    ep_count = lax.axis_size("ep")
    ep_index = lax.axis_index("ep")
    tp_index = lax.axis_index("tp")
    own_rows, model_width = tokens.shape
    head_count, head_size = (memory.shape[1], memory.shape[3])
    token_total, top_count = routes.shape
    local_experts = gate_proj.shape[0]
    experts_all = local_experts * ep_count
    capacity = max(2, 2 * own_rows * top_count // ep_count)
    slot_rows = ep_count * capacity
    tp_width = output_gain.shape[0]
    tokens_float = tokens.astype(jnp.float32)
    normed = (tokens_float * rms_scale(tokens_float) * mixer_gain).astype(jnp.bfloat16)
    log_input = jnp.einsum("sd,hd->sh", normed, igate_weight, preferred_element_type=jnp.float32)
    log_forget = jax.nn.log_sigmoid(
        jnp.einsum("sd,hd->sh", normed, fgate_weight, preferred_element_type=jnp.float32)
    )
    tokens_split = lax.all_to_all(tokens, "ep", split_axis=1, concat_axis=0, tiled=True)
    pieces = in_one_piece((query_weight, key_weight, value_weight, outgate_weight), "ep", 0, 1)
    projected_float = jnp.concatenate(
        [jnp.dot(normed, matrix, preferred_element_type=jnp.float32) for matrix in pieces], axis=1
    )
    projected = projected_float.astype(jnp.bfloat16)
    projected = (
        lax.optimization_barrier(projected)
        .astype(jnp.float32)
        .reshape(own_rows, 4, head_count, head_size)
    )
    gated_heads = read_memory(projected, log_input, log_forget, memory, stabilizer, head_gain)
    all_heads = gathered_copies(gated_heads, "tp", 1)
    mixed_rows = jnp.dot(
        lax.all_gather(all_heads, "ep", axis=0, tiled=True),
        down_weight,
        preferred_element_type=jnp.float32,
    )
    split_float = tokens_split.astype(jnp.float32)
    gained_rows = mixed_rows * mixed_gain
    mixed_squares, cross_sum, gained_squares, token_squares = packed_total(
        (
            jnp.sum(mixed_rows * mixed_rows, axis=-1),
            jnp.sum(split_float * gained_rows, axis=-1),
            jnp.sum(gained_rows * gained_rows, axis=-1),
            jnp.sum(split_float * split_float, axis=-1),
        ),
        "ep",
    )
    mixed_scale = lax.rsqrt(mixed_squares / model_width + NORM_EPS)
    residual_float = split_float + gained_rows * mixed_scale[:, None]
    residual_squares = (
        token_squares + 2.0 * mixed_scale * cross_sum + mixed_scale * mixed_scale * gained_squares
    )
    residual = residual_float.astype(jnp.bfloat16)
    expert_in = (
        residual_float * lax.rsqrt(residual_squares / model_width + NORM_EPS)[:, None] * expert_gain
    ).astype(jnp.bfloat16)
    residual_own = lax.all_to_all(residual, "ep", split_axis=0, concat_axis=1, tiled=True)
    residual_mine = lax.dynamic_slice_in_dim(residual_own, tp_index * tp_width, tp_width, 1)
    destination, slot_token = slot_tables(routes, ep_count, experts_all, capacity)
    slot_grid = slot_token.reshape(experts_all, slot_rows)
    padded_in = jnp.concatenate(
        [expert_in, jnp.zeros((1, expert_in.shape[1]), jnp.bfloat16)], axis=0
    )
    outgoing = padded_in[slot_grid]
    arrived = lax.all_to_all(outgoing, "ep", split_axis=0, concat_axis=2, tiled=True)
    partial_value = run_experts(arrived, gate_proj, up_proj, expert_down)
    reduced = sent_and_summed(partial_value.astype(jnp.bfloat16), "tp", 2)
    returned = lax.all_to_all(
        reduced.astype(jnp.bfloat16), "ep", split_axis=1, concat_axis=0, tiled=True
    ).astype(reduced.dtype)
    own_destination = lax.dynamic_slice_in_dim(destination, ep_index * own_rows, own_rows, 0)
    own_index = own_destination // slot_rows * capacity + own_destination % capacity
    picked = returned.reshape(experts_all * capacity, tp_width)[own_index]
    own_weight = lax.dynamic_slice_in_dim(route_weights, ep_index * own_rows, own_rows, 0)
    combined = jnp.sum(picked * own_weight[..., None], axis=1)
    combined_squares = taken_together(jnp.sum(combined * combined, axis=-1), "tp")
    final_rows = (
        residual_mine.astype(jnp.float32)
        + combined * lax.rsqrt(combined_squares / model_width + NORM_EPS)[:, None] * output_gain
    )
    return final_rows.astype(jnp.bfloat16)


def solution(mesh):
    placed = (
        P("ep", None),
        P(),
        P("ep", "tp"),
        P("ep", "tp"),
        P("ep", "tp"),
        P("ep", "tp"),
        P("tp", None),
        P("tp", None),
        P("ep", "tp", None, None),
        P("ep", "tp"),
        P("tp"),
        P(None, "ep"),
        P("ep"),
        P("ep"),
        P(),
        P(),
        P("ep", None, "tp"),
        P("ep", None, "tp"),
        P("ep", "tp", None),
        P("tp"),
    )
    return jax.shard_map(
        shards, mesh=mesh, in_specs=placed, out_specs=P("ep", "tp"), check_vma=False
    )
```

profile of v0, /device:TPU:1, one launch (start us, length us, event | category | flops | bytes accessed | tf_op | source)
XLA Modules:
  0.0 246.7 jit_solution(5439987400903227595)
XLA Ops:
  6.5 1.8 pad_maximum_fusion
  8.4 1.0 fusion.58
  9.4 1.1 bitcast_add_fusion
  10.5 55.6 %all-gather.3.cloned.1.call-done = bf16[2048,2048]{1,0:T(8,128)(2,1)} async-done(((bf16[64,2048]{1,0:T(8,128)(2,1)}), bf16[2048,2048]{1,0:T(8,128)(2,1)}) %all-gather.3.cloned.1.call-update) | async-done | bytes 8388624 | tf_op jit(solution)/shard_map/all_gather | solution.py:17
  66.1 2.1 fusion.39
  68.2 2.0 fusion.42
  70.2 2.0 fusion.45
  72.2 2.0 fusion.48
  74.4 0.2 fusion.74
  74.6 7.0 %fusion = f32[16,1,512]{2,1,0:T(1,128)S(1)} fusion(f32[16,4,1,512]{3,1,0,2:T(4,128)S(1)} %reshape.302, f32[16,1,512,512]{3,2,1,0:T(8,128)} %param.28), kind=kOutput, calls=%fused_computation.3 | convolution fusion | flops 8396800 | bytes 16842752 | tf_op jit(solution)/shard_map/nhd,nhde->nhe/dot_general | solution.py:97
  81.6 0.2 fusion.105
  82.3 8.2 %all_to_all.78 = bf16[4,16,512]{2,1,0:T(8,128)(2,1)S(1)} all-to-all(bf16[4,16,512]{2,1,0:T(8,128)(2,1)S(1)} %broadcast_in_dim.10), channel_id=1, replica_groups=mesh['ep'=32,'tp'=4] {'tp'}, dimensions={0} | all-to-all | bytes 131072 | tf_op jit(solution)/shard_map/all_to_all | solution.py:28
  90.6 0.6 copy.173
  91.5 0.7 reshape.342
  92.2 6.9 %all-to-all-start = ((bf16[32,2,512]{2,1,0:T(2,128)(2,1)}), bf16[32,2,512]{2,1,0:T(2,128)(2,1)S(1)}, u32[]{:S(2)}, u32[]{:S(2)}) async-start(bf16[32,2,512]{2,1,0:T(2,128)(2,1)} %reshape.342), calls=%async_computation | async-start | bytes 131072 | tf_op jit(solution)/shard_map/all_to_all | solution.py:162
  99.8 1.7 select_reduce_fusion
  101.8 4.7 %all-to-all-done = bf16[32,2,512]{2,1,0:T(2,128)(2,1)S(1)} async-done(((bf16[32,2,512]{2,1,0:T(2,128)(2,1)}), bf16[32,2,512]{2,1,0:T(2,128)(2,1)S(1)}, u32[]{:S(2)}, u32[]{:S(2)}) %all-to-all-start) | async-done | bytes 65568 | tf_op jit(solution)/shard_map/all_to_all | solution.py:162
  107.0 27.2 %all-gather.5.cloned.1.call-done = bf16[512,2048]{1,0:T(8,128)(2,1)} async-done(((bf16[16,2048]{1,0:T(8,128)(2,1)}), bf16[512,2048]{1,0:T(8,128)(2,1)}) %all-gather.5.cloned.1.call-update) | async-done | bytes 2097168 | tf_op jit(solution)/shard_map/all_gather | solution.py:176
  134.2 2.4 multiply_reduce_fusion.3
  136.6 0.8 broadcast_in_dim.11
  137.5 5.3 %all-to-all-start.2 = ((f32[32,1,2048]{2,1,0:T(1,128)}), f32[32,1,2048]{2,1,0:T(1,128)S(1)}, u32[]{:S(2)}, u32[]{:S(2)}) async-start(f32[32,1,2048]{2,1,0:T(1,128)} %broadcast_in_dim.11), calls=%async_computation.2 | async-start | bytes 524288 | tf_op jit(solution)/shard_map/all_to_all | solution.py:28
  142.8 8.1 %scatter_custom_fusion = s32[4096]{0:T(1024)S(1)} fusion(s32[2048]{0:T(1024)S(1)} %bitcast.145, s32[2048]{0:T(1024)S(1)} %add_select_fusion.2, s32[]{:T(128)} %constant.95.clone.1), kind=kCustom, calls=%fused_computation.110 | custom fusion | bytes 16388 | tf_op jit(solution)/shard_map/scatter | solution.py:82
  150.8 0.6 fusion.76
  151.8 0.7 fusion.77
  152.7 14.1 %gather_fusion = bf16[4096,64]{1,0:T(8,128)(2,1)S(1)} fusion(bf16[513,64]{1,0:T(8,128)(2,1)S(1)} %concatenate.16.clone, s32[4096]{0:T(1024)} %fusion.76), kind=kCustom, calls=%fused_computation | custom fusion | bytes 1064960 | tf_op jit(solution)/shard_map/gather | solution.py:207
  166.8 1.1 copy.156
  167.9 18.6 %all_to_all.79 = bf16[32,128,64]{1,2,0:T(8,128)(2,1)S(1)} all-to-all(bf16[32,128,64]{1,2,0:T(8,128)(2,1)} %copy.156), channel_id=1, replica_groups=mesh['ep'=32,'tp'=4] {'ep'}, dimensions={0} | all-to-all | bytes 1048576 | tf_op jit(solution)/shard_map/all_to_all | solution.py:208
  186.6 2.8 %fusion.22 = f32[128,512]{1,0:T(8,128)} fusion(bf16[128,2048]{0,1:T(8,128)(2,1)S(1)} %bitcast.131, bf16[1,2048,512]{2,1,0:T(8,128)(2,1)} %param.36), kind=kOutput, calls=%fused_computation.23 | convolution fusion | flops 268500992 | bytes 2883584 | tf_op jit(solution)/shard_map/erd,edh->erh/dot_general | solution.py:109
  189.3 2.5 %convolution_convert_fusion = bf16[128,2048]{1,0:T(8,128)(2,1)S(1)} fusion(bf16[1,512,2048]{2,1,0:T(8,128)(2,1)S(1)} %copy-done, f32[128,512]{1,0:T(8,128)} %fusion.22, bf16[128,2048]{0,1:T(8,128)(2,1)S(1)} %bitcast.132, bf16[1,2048,512]{2,1,0:T(8,128)(2,1)} %param.37), kind=kOutput, calls=%fused_computation.5 | convolution fusion | flops 537722880 | bytes 5505024 | tf_op jit(solution)/shard_map/erh,ehd->erd/dot_general | solution.py:120
  191.8 0.4 reshape.299
  192.2 0.9 copy.199
  193.1 4.0 %all-to-all-start.5 = ((bf16[4,1,128,512]{3,2,1,0:T(8,128)(2,1)}), bf16[4,1,128,512]{3,2,1,0:T(8,128)(2,1)S(1)}, u32[]{:S(2)}, u32[]{:S(2)}) async-start(bf16[4,1,128,512]{3,2,1,0:T(8,128)(2,1)} %bitcast.128), calls=%async_computation.5 | async-start | bytes 1048576 | tf_op jit(solution)/shard_map/all_to_all | solution.py:57
  197.5 0.8 reshape.346
  198.3 7.7 %all-to-all-done.5 = bf16[4,1,128,512]{3,2,1,0:T(8,128)(2,1)S(1)} async-done(((bf16[4,1,128,512]{3,2,1,0:T(8,128)(2,1)}), bf16[4,1,128,512]{3,2,1,0:T(8,128)(2,1)S(1)}, u32[]{:S(2)}, u32[]{:S(2)}) %all-to-all-start.5) | async-done | bytes 524320 | tf_op jit(solution)/shard_map/all_to_all | solution.py:57
  205.9 5.2 %all-to-all-start.3 = ((bf16[32,2,512]{2,1,0:T(2,128)(2,1)}), bf16[32,2,512]{2,1,0:T(2,128)(2,1)S(1)}, u32[]{:S(2)}, u32[]{:S(2)}) async-start(bf16[32,2,512]{2,1,0:T(2,128)(2,1)} %reshape.346), calls=%async_computation.3 | async-start | bytes 131072 | tf_op jit(solution)/shard_map/all_to_all | solution.py:200
  211.4 0.2 copy.200
  211.6 0.5 broadcast.232
  212.1 1.4 reduce.12
  213.5 0.7 reshape.344
  214.3 4.4 %all-to-all-done.3 = bf16[32,2,512]{2,1,0:T(2,128)(2,1)S(1)} async-done(((bf16[32,2,512]{2,1,0:T(2,128)(2,1)}), bf16[32,2,512]{2,1,0:T(2,128)(2,1)S(1)}, u32[]{:S(2)}, u32[]{:S(2)}) %all-to-all-start.3) | async-done | bytes 65568 | tf_op jit(solution)/shard_map/all_to_all | solution.py:200
  218.6 3.9 %all-to-all-start.6 = ((bf16[32,2,1024]{2,1,0:T(2,128)(2,1)}), bf16[32,2,1024]{2,1,0:T(2,128)(2,1)S(1)}, u32[]{:S(2)}, u32[]{:S(2)}) async-start(bf16[32,2,1024]{2,1,0:T(2,128)(2,1)} %reshape.344), calls=%async_computation.6 | async-start | bytes 262144 | tf_op jit(solution)/shard_map/all_to_all | solution.py:211
  222.5 0.8 constant_dynamic-slice_fusion
  223.6 6.6 %all-to-all-done.6 = bf16[32,2,1024]{2,1,0:T(2,128)(2,1)S(1)} async-done(((bf16[32,2,1024]{2,1,0:T(2,128)(2,1)}), bf16[32,2,1024]{2,1,0:T(2,128)(2,1)S(1)}, u32[]{:S(2)}, u32[]{:S(2)}) %all-to-all-start.6) | async-done | bytes 131104 | tf_op jit(solution)/shard_map/all_to_all | solution.py:211
  230.4 0.7 gather_fusion.1
  231.3 0.6 broadcast_in_dim.14
  231.9 3.2 %all-to-all-start.7 = ((f32[4,1,16]{2,1,0:T(1,128)}), f32[4,1,16]{2,1,0:T(1,128)S(1)}, u32[]{:S(2)}, u32[]{:S(2)}) async-start(f32[4,1,16]{2,1,0:T(1,128)} %broadcast_in_dim.14), calls=%async_computation.7 | async-start | bytes 4096 | tf_op jit(solution)/shard_map/all_to_all | solution.py:28
  235.4 3.8 %all-to-all-done.7 = f32[4,1,16]{2,1,0:T(1,128)S(1)} async-done(((f32[4,1,16]{2,1,0:T(1,128)}), f32[4,1,16]{2,1,0:T(1,128)S(1)}, u32[]{:S(2)}, u32[]{:S(2)}) %all-to-all-start.7) | async-done | bytes 288 | tf_op jit(solution)/shard_map/all_to_all | solution.py:28
  239.2 0.7 add_convert_fusion
  (83 shorter events, 4.4 us)
Async XLA Ops:
  6.5 182.8 %copy-start = (bf16[1,512,2048]{2,1,0:T(8,128)(2,1)S(1)}, bf16[1,512,2048]{2,1,0:T(8,128)(2,1)}, u32[]{:S(2)}) copy-start(bf16[1,512,2048]{2,1,0:T(8,128)(2,1)} %param.38) | copy-start | bytes 6291460
  6.5 61.7 %copy-start.3 = (bf16[16,2048]{1,0:T(8,128)(2,1)S(1)}, bf16[16,2048]{1,0:T(8,128)(2,1)}, u32[]{:S(2)}) copy-start(bf16[16,2048]{1,0:T(8,128)(2,1)} %param.20) | copy-start | bytes 196612
  6.5 61.7 %copy-start.11 = (f32[2048]{0:T(1024)S(1)}, f32[2048]{0:T(1024)}, u32[]{:S(2)}) copy-start(f32[2048]{0:T(1024)} %param.21) | copy-start | bytes 24580
  6.5 59.6 %all-gather.3.cloned.1.call-start = ((), (), s32[]{:S(2)}) async-start(), calls=%async_computation.8 | async-start | bytes 8650752 | tf_op jit(solution)/shard_map/all_gather | solution.py:17
  8.4 125.8 %all-gather.5.cloned.1.call-start = ((), (), s32[]{:S(2)}) async-start(), calls=%async_computation.9 | async-start | bytes 2162688 | tf_op jit(solution)/shard_map/all_gather | solution.py:176
  74.6 7.0 %copy-start.12 = (bf16[1,2048]{1,0:T(2,128)(2,1)S(1)}, bf16[1,2048]{1,0:T(2,128)(2,1)}, u32[]{:S(2)}) copy-start(bf16[1,2048]{1,0:T(2,128)(2,1)} %param.26) | copy-start | bytes 12292
  74.6 7.6 %copy-start.8 = (f32[512]{0:T(512)S(1)}, f32[512]{0:T(512)}, u32[]{:S(2)}) copy-start(f32[512]{0:T(512)} %param.30) | copy-start | bytes 6148
  74.6 24.6 %copy-start.6 = (s32[512,4]{0,1:T(4,128)S(1)}, s32[512,4]{0,1:T(4,128)}, u32[]{:S(2)}) copy-start(s32[512,4]{0,1:T(4,128)} %param.34) | copy-start | bytes 24580
  81.8 52.4 %copy-start.1 = (bf16[2048,64]{0,1:T(8,128)(2,1)S(1)}, bf16[2048,64]{0,1:T(8,128)(2,1)}, u32[]{:S(2)}) copy-start(bf16[2048,64]{0,1:T(8,128)(2,1)} %param.31) | copy-start | bytes 786436
  81.8 52.4 %copy-start.7 = (f32[64]{0:T(128)S(1)}, f32[64]{0:T(128)}, u32[]{:S(2)}) copy-start(f32[64]{0:T(128)} %param.32) | copy-start | bytes 772
  92.2 14.3 %all-to-all-start = ((bf16[32,2,512]{2,1,0:T(2,128)(2,1)}), bf16[32,2,512]{2,1,0:T(2,128)(2,1)S(1)}, u32[]{:S(2)}, u32[]{:S(2)}) async-start(bf16[32,2,512]{2,1,0:T(2,128)(2,1)} %reshape.342), calls=%async_computation | async-start | bytes 131072 | tf_op jit(solution)/shard_map/all_to_all | solution.py:162
  101.5 4.9 %copy-start.4 = (s32[32,64]{1,0:T(8,128)}, s32[32,64]{1,0:T(8,128)S(1)}, u32[]{:S(2)}) copy-start(s32[32,64]{1,0:T(8,128)S(1)} %copy.154) | copy-start | bytes 24580
  106.7 45.2 %copy-start.10 = (f32[64]{0:T(128)S(1)}, f32[64]{0:T(128)}, u32[]{:S(2)}) copy-start(f32[64]{0:T(128)} %param.33) | copy-start | bytes 772
  137.5 14.2 %all-to-all-start.2 = ((f32[32,1,2048]{2,1,0:T(1,128)}), f32[32,1,2048]{2,1,0:T(1,128)S(1)}, u32[]{:S(2)}, u32[]{:S(2)}) async-start(f32[32,1,2048]{2,1,0:T(1,128)} %broadcast_in_dim.11), calls=%async_computation.2 | async-start | bytes 524288 | tf_op jit(solution)/shard_map/all_to_all | solution.py:28
  191.8 5.3 %copy-start.5 = (s32[32,64]{1,0:T(8,128)S(1)}, s32[32,64]{1,0:T(8,128)}, u32[]{:S(2)}) copy-start(s32[32,64]{1,0:T(8,128)} %copy-done.4) | copy-start | bytes 24580
  191.8 5.6 %copy-start.2 = (bf16[512,64]{0,1:T(8,128)(2,1)S(1)}, bf16[512,64]{0,1:T(8,128)(2,1)}, u32[]{:S(2)}) copy-start(bf16[512,64]{0,1:T(8,128)(2,1)} %get-tuple-element.10) | copy-start | bytes 196612
  193.1 12.9 %all-to-all-start.5 = ((bf16[4,1,128,512]{3,2,1,0:T(8,128)(2,1)}), bf16[4,1,128,512]{3,2,1,0:T(8,128)(2,1)S(1)}, u32[]{:S(2)}, u32[]{:S(2)}) async-start(bf16[4,1,128,512]{3,2,1,0:T(8,128)(2,1)} %bitcast.128), calls=%async_computation.5 | async-start | bytes 1048576 | tf_op jit(solution)/shard_map/all_to_all | solution.py:57
  205.9 12.7 %all-to-all-start.3 = ((bf16[32,2,512]{2,1,0:T(2,128)(2,1)}), bf16[32,2,512]{2,1,0:T(2,128)(2,1)S(1)}, u32[]{:S(2)}, u32[]{:S(2)}) async-start(bf16[32,2,512]{2,1,0:T(2,128)(2,1)} %reshape.346), calls=%async_computation.3 | async-start | bytes 131072 | tf_op jit(solution)/shard_map/all_to_all | solution.py:200
  212.1 27.1 %copy-start.9 = (f32[512]{0:T(512)S(1)}, f32[512]{0:T(512)}, u32[]{:S(2)}) copy-start(f32[512]{0:T(512)} %param.39) | copy-start | bytes 6148
  218.6 11.6 %all-to-all-start.6 = ((bf16[32,2,1024]{2,1,0:T(2,128)(2,1)}), bf16[32,2,1024]{2,1,0:T(2,128)(2,1)S(1)}, u32[]{:S(2)}, u32[]{:S(2)}) async-start(bf16[32,2,1024]{2,1,0:T(2,128)(2,1)} %reshape.344), calls=%async_computation.6 | async-start | bytes 262144 | tf_op jit(solution)/shard_map/all_to_all | solution.py:211
  231.9 7.3 %all-to-all-start.7 = ((f32[4,1,16]{2,1,0:T(1,128)}), f32[4,1,16]{2,1,0:T(1,128)S(1)}, u32[]{:S(2)}, u32[]{:S(2)}) async-start(f32[4,1,16]{2,1,0:T(1,128)} %broadcast_in_dim.14), calls=%async_computation.7 | async-start | bytes 4096 | tf_op jit(solution)/shard_map/all_to_all | solution.py:28
Sparse Core Ops, SparseCore 0:
  9.6 56.4 all-gather.2
  91.3 42.8 all-gather.4
where the time goes:
time: 248 us; the launch traced here: 247 us
  waiting for transfers between devices  110 us (44%)
  local copies, waits for them, and re-layouts  33.7 us (14%)
  starting transfers between devices  28.6 us (12%)
  blocking collectives  26.9 us (11%)
  matrix products  24 us (10%)
  between operations  13.8 us (6%)
  other arithmetic  9.5 us (4%)
    all_gather x1, waiting for transfers between devices, in_one_piece(): lax.all_gather(both, axis, axis=dim, tiled=True)  55.6 us
    all_gather x1, waiting for transfers between devices, shards(): lax.all_gather(all_heads, 'ep', axis=0, tiled=True)  27.2 us
    all_to_all x1, blocking collectives, shards(): lax.all_to_all(outgoing, 'ep', split_axis=0, concat_axis=2, tiled=True)  18.6 us
    gather x2, local copies, waits for them, and re-layouts, shards(): outgoing = padded_in[slot_grid]  15.2 us
    all_to_all x2, starting transfers between devices, copy_for_each(): lax.all_to_all(jnp.broadcast_to(shard[None], (devices, *shard.shape)), ax...  8.52 us
    all_to_all x1, blocking collectives, copy_for_each(): lax.all_to_all(jnp.broadcast_to(shard[None], (devices, *shard.shape)), ax...  8.25 us
    dot_general x4, matrix products, shards(): jnp.dot(normed, matrix, preferred_element_type=jnp.float32)  8.11 us
    scatter x1, local copies, waits for them, and re-layouts, slot_tables(): slot_token = jnp.full((experts * groups * capacity,), token_total, jnp.in...  8.06 us
  transfers between devices with their start and end apart: 8, of which 8 were waited for; matrix products, arithmetic and copies ran while one was open for 8% of the time, Pallas kernels for 0%

commit v1 on v0

v1 whole, which is shorter than its diff:
```python
import functools
import jax
import jax.numpy as jnp
from jax import lax
from jax.experimental import pallas as pl
from jax.experimental.pallas import tpu as pltpu
from jax.sharding import PartitionSpec as P

EPS = 1e-06
LIMIT = 7.0
SIG = 1.702
F32 = jnp.float32
BF16 = jnp.bfloat16
N_REMOTE = 96
N_LOCAL = 48


def iota(shape, dim):
    return lax.broadcasted_iota(jnp.int32, shape, dim)


def sigmoid(x):
    return 1.0 / (1.0 + jnp.exp(-x))


def mm(a, b):
    return jnp.dot(a, b, preferred_element_type=F32)


def body(
    tok_h, mixg_h, wq_h, wk_h, wv_h, wo_h, ig_h, fg_h, mem_h, stab_h, hg_h, dw_h,
    mg_h, eg_h, rt_h, rw_h, w1_h, w3_h, w2_h, og_h,
    out,
    tok, mixg, wa, wb, ig, fg, mem, stab, hg, dt, mg, eg, gains, rt, rw, w1, w3, w2, og,
    nrm, na, xa, xb, sa, sb, ra, rb, sa2, sb2, ra2, rb2, qpad, qt, read,
    mx, gfull, resid, xst, oh_s, ohw_hi, ohw_lo, perm, permt,
    do, di, yst, act, sx, rx, own_x, rst, zo, zi, sq,
    ss, rs, ls, a2a_s, a2a_r,
):
    ep = lax.axis_index("ep")
    t = lax.axis_index("tp")
    z = ep // 8
    y = (ep // 2) % 4
    c = ep % 2
    partner = {"ep": z * 8 + y * 2 + (1 - c)}

    def zdev(zz):
        return {"ep": zz * 8 + y * 2 + c}

    def ydev(yy):
        return {"ep": z * 8 + yy * 2 + c}

    def xdev(xx):
        return {"tp": xx}

    count = [0, 0]
    sent = []

    def rcopy(src, dst, dev):
        i = count[0]
        count[0] += 1
        cp = pltpu.make_async_remote_copy(
            src_ref=src, dst_ref=dst, send_sem=ss.at[i], recv_sem=rs.at[i],
            device_id=dev, device_id_type=pl.DeviceIdType.MESH,
        )
        cp.start()
        sent.append(cp)
        return cp

    def lcopy(src, dst):
        i = count[1]
        count[1] += 1
        cp = pltpu.make_async_copy(src, dst, ls.at[i])
        cp.start()
        return cp

    l_tok = lcopy(tok_h, tok)
    l_mixg = lcopy(mixg_h, mixg)
    l_w = [
        lcopy(wq_h, wa.at[0, z, c]), lcopy(wv_h, wa.at[1, z, c]),
        lcopy(wk_h, wb.at[0, y, c]), lcopy(wo_h, wb.at[1, y, c]),
    ]
    l_g = [lcopy(mg_h, mg), lcopy(eg_h, eg)]
    l_small = [
        lcopy(ig_h, ig), lcopy(fg_h, fg), lcopy(stab_h, stab), lcopy(hg_h, hg),
        lcopy(rt_h, rt), lcopy(rw_h, rw), lcopy(og_h, og),
    ]
    own_rows = pl.ds(pl.multiple_of(t * 512, 512), 512)
    l_dw = lcopy(dw_h.at[:, own_rows], dt.at[z, y, c])

    bar = pltpu.get_barrier_semaphore()
    near = [partner]
    for d in (1, 2, 3):
        near += [zdev((z + d) % 4), ydev((y + d) % 4), xdev((t + d) % 4)]
    for dev in near:
        pl.semaphore_signal(bar, inc=1, device_id=dev, device_id_type=pl.DeviceIdType.MESH)
    pl.semaphore_wait(bar, len(near))

    a_in, b_in = {}, {}
    for d in (2, 1, 3):
        zz, yy = (z + d) % 4, (y + d) % 4
        a_in[d] = [
            rcopy(wq_h, wa.at[0, z, c], zdev(zz)), rcopy(wv_h, wa.at[1, z, c], zdev(zz)),
        ]
        b_in[d] = [
            rcopy(wk_h, wb.at[0, y, c], ydev(yy)), rcopy(wo_h, wb.at[1, y, c], ydev(yy)),
        ]
    p_in = [
        rcopy(wq_h, wa.at[0, z, c], partner), rcopy(wv_h, wa.at[1, z, c], partner),
        rcopy(wk_h, wb.at[0, y, c], partner), rcopy(wo_h, wb.at[1, y, c], partner),
    ]
    l_mem = [lcopy(mem_h.at[pl.ds(2 * i, 2), 0], mem.at[pl.ds(2 * i, 2)]) for i in range(8)]
    l_exp = [lcopy(w1_h.at[0], w1), lcopy(w3_h.at[0], w3), lcopy(w2_h.at[0], w2)]

    l_tok.wait()
    l_mixg.wait()
    x = tok[...].astype(F32)
    ms = jnp.mean(x * x, axis=-1, keepdims=True)
    normed = (x * lax.rsqrt(ms + EPS) * mixg[...]).astype(BF16)
    nrm[...] = normed
    for yy in range(4):
        for zz in range(4):
            na[yy, :, zz * 128:(zz + 1) * 128] = normed[:, zz * 512 + yy * 128:zz * 512 + yy * 128 + 128]
    xa[y] = na[y]
    xb[z] = nrm[:, pl.ds(pl.multiple_of(z * 512, 512), 512)]
    ta_in, tb_in = [], []
    for d in (2, 1, 3):
        zz, yy = (z + d) % 4, (y + d) % 4
        ta_in.append(rcopy(na.at[yy], xa.at[y], ydev(yy)))
        tb_in.append(rcopy(nrm.at[:, pl.ds(pl.multiple_of(zz * 512, 512), 512)], xb.at[z], zdev(zz)))

    da_in, db_in = [], []
    for d in (2, 1, 3):
        zz, yy = (z + d) % 4, (y + d) % 4
        lo = pl.ds(pl.multiple_of(t * 512, 256), 256)
        hi = pl.ds(pl.multiple_of(t * 512 + 256, 256), 256)
        da_in.append(rcopy(dw_h.at[:, lo], dt.at[z, y, c, :, 0:256], zdev(zz)))
        db_in.append(rcopy(dw_h.at[:, hi], dt.at[z, y, c, :, 256:512], ydev(yy)))

    for cp in l_g:
        cp.wait()
    spread = ((iota((64, 128), 1) & 63) == iota((64, 128), 0)).astype(F32)
    mg128 = jnp.dot(jnp.broadcast_to(mg[...], (8, 64)), spread, precision=lax.Precision.HIGHEST, preferred_element_type=F32)
    eg128 = jnp.dot(jnp.broadcast_to(eg[...], (8, 64)), spread, precision=lax.Precision.HIGHEST, preferred_element_type=F32)
    gains[z, y, c] = jnp.where(iota((8, 128), 0) == 0, mg128, eg128)
    g1_in = [rcopy(gains.at[z, y, c], gains.at[z, y, c], zdev((z + d) % 4)) for d in (2, 1, 3)]

    for cp in l_small:
        cp.wait()
    nf = normed.astype(F32)
    log_in = jnp.sum(nf * ig[...].astype(F32), axis=-1, keepdims=True)
    pre_f = jnp.sum(nf * fg[...].astype(F32), axis=-1, keepdims=True)
    log_f = jnp.minimum(pre_f, 0.0) - jnp.log(1.0 + jnp.exp(-jnp.abs(pre_f)))
    eye = iota((16, 16), 0) == iota((16, 16), 1)
    st = jnp.sum(jnp.where(eye, jnp.broadcast_to(stab[...], (16, 16)), 0.0), axis=-1, keepdims=True)
    peak = jnp.maximum(log_f + st, log_in)
    within = jnp.exp(log_in - peak)
    carried = jnp.exp(log_f + st - peak)

    sel = (iota((64, 512), 1) == ep * 16 + (iota((64, 512), 0) & 15))
    col = iota((64, 512), 1)
    cx = jnp.zeros((64, 512), F32)
    wx = jnp.zeros((64, 512), F32)
    for k in range(4):
        r_k = jnp.sum(jnp.where(sel, rt[k:k + 1, :], 0), axis=-1, keepdims=True)
        w_k = jnp.sum(jnp.where(sel, rw[k:k + 1, :], 0.0), axis=-1, keepdims=True)
        hit = ((col >> 4) == r_k).astype(F32)
        cx = cx + hit
        wx = wx + hit * w_k
    r64, c64 = iota((64, 64), 0), iota((64, 64), 1)
    lower = (((r64 >> 4) == (c64 >> 4)) & (c64 < r64)).astype(BF16)
    before = mm(lower, cx.astype(BF16))
    fits = (before == (col & 3).astype(F32)) & (((col >> 2) & 3) == (iota((64, 512), 0) >> 4))
    oh = jnp.where(fits, cx, 0.0)
    oh_s[...] = jnp.transpose(oh).astype(BF16)
    ohw = oh * wx
    hi_part = ohw.astype(BF16)
    ohw_hi[...] = hi_part
    ohw_lo[...] = (ohw - hi_part.astype(F32)).astype(BF16)
    r5, c5 = iota((512, 512), 0), iota((512, 512), 1)
    perm[...] = (c5 == 16 * ((r5 & 127) >> 2) + 4 * (r5 >> 7) + (r5 & 3)).astype(BF16)
    permt[...] = (r5 == 16 * ((c5 & 127) >> 2) + 4 * (c5 >> 7) + (c5 & 3)).astype(BF16)

    f_in = []
    for n, d in enumerate((1, 3, 2)):
        zz, yy = (z + 4 - d) % 4, (y + 4 - d) % 4
        for cp in a_in[d]:
            cp.wait_recv()
        f_in.append(rcopy(wa.at[:, zz, c], wa.at[:, zz, c], partner))
        for cp in b_in[d]:
            cp.wait_recv()
        f_in.append(rcopy(wb.at[:, yy, c], wb.at[:, yy, c], partner))
    for cp in ta_in + tb_in:
        cp.wait_recv()
    for cp in l_w:
        cp.wait()
    for cp in p_in + f_in:
        cp.wait_recv()

    ax = xa[...].reshape(64, 512)
    bx = xb[...].reshape(64, 512)
    sa[...] = mm(ax, wa[0].reshape(512, 512)).reshape(4, 16, 512)
    sb[...] = mm(bx, wb[0].reshape(512, 512)).reshape(4, 16, 512)
    pr_in = []
    for d in (2, 1, 3):
        zz, yy = (z + d) % 4, (y + d) % 4
        pr_in.append(rcopy(sa.at[yy], ra.at[y], ydev(yy)))
        pr_in.append(rcopy(sb.at[zz], rb.at[z], zdev(zz)))
    sa2[...] = mm(ax, wa[1].reshape(512, 512)).astype(BF16).reshape(4, 16, 512)
    sb2[...] = mm(bx, wb[1].reshape(512, 512)).astype(BF16).reshape(4, 16, 512)
    for d in (2, 1, 3):
        zz, yy = (z + d) % 4, (y + d) % 4
        pr_in.append(rcopy(sa2.at[yy], ra2.at[y], ydev(yy)))
        pr_in.append(rcopy(sb2.at[zz], rb2.at[z], zdev(zz)))
    ra[y] = sa[y]
    rb[z] = sb[z]
    ra2[y] = sa2[y]
    rb2[z] = sb2[z]

    l_dw.wait()
    for cp in da_in + db_in + g1_in:
        cp.wait_recv()
    d2_in = []
    for d in (2, 1, 3):
        zz, yy = (z + d) % 4, (y + d) % 4
        d2_in.append(rcopy(gains.at[:, y, c], gains.at[:, y, c], ydev(yy)))
        d2_in.append(rcopy(dt.at[:, y, c, :, 0:256], dt.at[:, y, c, :, 0:256], ydev(yy)))
        d2_in.append(rcopy(dt.at[z, :, c, :, 256:512], dt.at[z, :, c, :, 256:512], zdev(zz)))

    for cp in pr_in:
        cp.wait_recv()
    q = jnp.sum(ra[...], axis=0).astype(BF16).astype(F32) * (512.0 ** -0.5)
    key = jnp.sum(rb[...], axis=0).astype(BF16).astype(F32)
    val = jnp.sum(ra2[...].astype(F32), axis=0)
    og_pre = jnp.sum(rb2[...].astype(F32), axis=0)
    qpad[0:16, :] = q
    qpad[16:128, :] = jnp.zeros((112, 512), F32)
    qt[...] = jnp.transpose(qpad[...])
    for cp in l_mem:
        cp.wait()
    for n in range(16):
        qcol = qt[:, n:n + 1]
        read[n:n + 1, :] = jnp.sum(qcol * mem[n], axis=0, keepdims=True)

    for cp in d2_in:
        cp.wait_recv()
    d3_in = [
        rcopy(dt.at[:, :, c], dt.at[:, :, c], partner),
        rcopy(gains.at[:, :, c], gains.at[:, :, c], partner),
    ]
    score = jnp.sum(q * key, axis=-1, keepdims=True) * within
    rd = score * val + carried * read[...]
    mean = jnp.mean(rd, axis=-1, keepdims=True)
    cen = rd - mean
    var = jnp.mean(cen * cen, axis=-1, keepdims=True)
    gated = (cen * lax.rsqrt(var + EPS) * hg[...] * sigmoid(og_pre)).astype(BF16)
    for cp in d3_in:
        cp.wait_recv()

    part = lax.dot_general(
        gated, dt[...].reshape(2048, 512), (((1,), (1,)), ((), ())), preferred_element_type=F32
    )
    mx[t] = part.astype(BF16)
    m_in = [rcopy(mx.at[t], mx.at[t], xdev((t + d) % 4)) for d in (2, 1, 3)]
    low = iota((1, 128), 1) < 64
    for zz in range(4):
        for yy in range(4):
            at = zz * 512 + yy * 128
            g0, g1 = gains[zz, yy, 0], gains[zz, yy, 1]
            gfull[:, at:at + 128] = jnp.where(low, g0, g1)
    for cp in m_in:
        cp.wait_recv()
    mixed = jnp.sum(mx[...].astype(F32), axis=0)
    xf = tok[...].astype(F32)
    mixed_gain = gfull[0:1, :]
    expert_gain = gfull[1:2, :]
    rf = xf + mixed * lax.rsqrt(jnp.mean(mixed * mixed, axis=-1, keepdims=True) + EPS) * mixed_gain
    resid[...] = rf.astype(BF16)
    ein = (rf * lax.rsqrt(jnp.mean(rf * rf, axis=-1, keepdims=True) + EPS) * expert_gain).astype(BF16)
    for k in range(4):
        xst[k * 16:(k + 1) * 16, :] = ein[:, k * 512:(k + 1) * 512]

    do[...] = mm(oh_s[...], xst[...]).astype(BF16)

    def peer_of(i):
        zz = (z + i // 8 + 2) % 4
        yy = (y + (i // 2) % 4 + 2) % 4
        cc = (c + i % 2) % 2
        return zz * 8 + yy * 2 + cc

    me16 = pl.ds(pl.multiple_of(ep * 16, 16), 16)

    def exchange(src, dst, k):
        def one(i, _):
            p = peer_of(i)
            rows = pl.ds(pl.multiple_of(p * 16, 16), 16)

            @pl.when(p != ep)
            def _():
                pltpu.make_async_remote_copy(
                    src_ref=src.at[rows, :], dst_ref=dst.at[me16, :],
                    send_sem=a2a_s.at[k], recv_sem=a2a_r.at[k],
                    device_id={"ep": p}, device_id_type=pl.DeviceIdType.MESH,
                ).start()
            return 0

        lax.fori_loop(0, 32, one, 0)
        dst[me16, :] = src[me16, :]
        return pltpu.make_async_remote_copy(
            src_ref=src.at[0:496, :], dst_ref=dst.at[0:496, :],
            send_sem=a2a_s.at[k], recv_sem=a2a_r.at[k],
            device_id=partner, device_id_type=pl.DeviceIdType.MESH,
        )

    ex1 = exchange(do, di, 0)
    for cp in l_exp:
        cp.wait()
    ex1.wait_recv()
    yst[...] = mm(perm[...], di[...]).astype(BF16)
    gate = jnp.zeros((128, 512), F32)
    up = jnp.zeros((128, 512), F32)
    for k in range(4):
        rows = yst[k * 128:(k + 1) * 128, :]
        gate = gate + mm(rows, w1[k * 512:(k + 1) * 512, :])
        up = up + mm(rows, w3[k * 512:(k + 1) * 512, :])
    gate = jnp.minimum(gate, LIMIT)
    up = jnp.clip(up, -LIMIT, LIMIT)
    act[...] = ((up + 1.0) * gate * sigmoid(SIG * gate)).astype(BF16)
    x_in = []
    for d in (2, 1, 3):
        tt = (t + d) % 4
        blk = mm(act[...], w2[:, pl.ds(pl.multiple_of(tt * 512, 512), 512)])
        sx[d - 1] = blk.astype(BF16)
        x_in.append(rcopy(sx.at[d - 1], rx.at[d - 1], xdev(tt)))
    own_x[...] = mm(act[...], w2[:, own_rows])
    for cp in x_in:
        cp.wait_recv()
    red = own_x[...] + jnp.sum(rx[...].astype(F32), axis=0)
    redb = red.astype(BF16)
    for k in range(4):
        rst[k * 128:(k + 1) * 128, :] = redb[:, k * 128:(k + 1) * 128]
    zo[...] = mm(permt[...], rst[...]).astype(BF16)
    ex2 = exchange(zo, zi, 1)
    ex2.wait_recv()
    comb4 = mm(ohw_hi[...], zi[...]) + mm(ohw_lo[...], zi[...])
    comb = jnp.concatenate([comb4[k * 16:(k + 1) * 16, :] for k in range(4)], axis=1)
    sq[t] = jnp.broadcast_to(jnp.sum(comb * comb, axis=-1, keepdims=True), (16, 128))
    s_in = [rcopy(sq.at[t], sq.at[t], xdev((t + d) % 4)) for d in (2, 1, 3)]
    for cp in s_in:
        cp.wait_recv()
    total = jnp.sum(sq[...], axis=0)[:, 0:1]
    mine = resid[:, own_rows].astype(F32)
    out[...] = (mine + comb * lax.rsqrt(total * (1.0 / 2048.0) + EPS) * og[...]).astype(BF16)
    for cp in sent:
        cp.wait_send()
    ex1.wait_send()
    ex2.wait_send()


def shards(
    tokens, mixer_gain, query_weight, key_weight, value_weight, outgate_weight,
    igate_weight, fgate_weight, memory, stabilizer, head_gain, down_weight,
    mixed_gain, expert_gain, routes, route_weights, gate_proj, up_proj, expert_down, output_gain,
):
    V = pltpu.VMEM
    scratch = [
        V((16, 2048), BF16), V((1, 2048), F32),
        V((2, 4, 2, 64, 512), BF16), V((2, 4, 2, 64, 512), BF16),
        V((1, 2048), BF16), V((1, 2048), BF16),
        V((16, 512, 512), F32), V((1, 16), F32), V((1, 512), F32),
        V((4, 4, 2, 64, 512), BF16),
        V((1, 64), F32), V((1, 64), F32), V((4, 4, 2, 8, 128), F32),
        V((4, 512), jnp.int32), V((4, 512), F32),
        V((2048, 512), BF16), V((2048, 512), BF16), V((512, 2048), BF16), V((1, 512), F32),
        V((16, 2048), BF16), V((4, 16, 512), BF16), V((4, 16, 512), BF16), V((4, 16, 512), BF16),
        V((4, 16, 512), F32), V((4, 16, 512), F32), V((4, 16, 512), F32), V((4, 16, 512), F32),
        V((4, 16, 512), BF16), V((4, 16, 512), BF16), V((4, 16, 512), BF16), V((4, 16, 512), BF16),
        V((128, 512), F32), V((512, 128), F32), V((16, 512), F32),
        V((4, 16, 2048), BF16), V((8, 2048), F32), V((16, 2048), BF16), V((64, 512), BF16),
        V((512, 64), BF16), V((64, 512), BF16), V((64, 512), BF16),
        V((512, 512), BF16), V((512, 512), BF16),
        V((512, 512), BF16), V((512, 512), BF16), V((512, 512), BF16), V((128, 512), BF16),
        V((3, 128, 512), BF16), V((3, 128, 512), BF16), V((128, 512), F32), V((512, 128), BF16),
        V((512, 128), BF16), V((512, 128), BF16), V((4, 16, 128), F32),
        pltpu.SemaphoreType.DMA((N_REMOTE,)), pltpu.SemaphoreType.DMA((N_REMOTE,)),
        pltpu.SemaphoreType.DMA((N_LOCAL,)),
        pltpu.SemaphoreType.DMA((2,)), pltpu.SemaphoreType.DMA((2,)),
    ]
    return pl.pallas_call(
        body,
        out_shape=jax.ShapeDtypeStruct((16, 512), BF16),
        in_specs=[pl.BlockSpec(memory_space=pl.ANY)] * 20,
        out_specs=pl.BlockSpec(memory_space=pltpu.VMEM),
        scratch_shapes=scratch,
        compiler_params=pltpu.CompilerParams(
            collective_id=0, has_side_effects=True, vmem_limit_bytes=56 * 1024 * 1024
        ),
        name="step",
    )(
        tokens, mixer_gain.reshape(1, 2048), query_weight, key_weight, value_weight, outgate_weight,
        igate_weight, fgate_weight, memory, stabilizer.T, head_gain.reshape(1, 512), down_weight.T,
        mixed_gain.reshape(1, 64), expert_gain.reshape(1, 64), routes.T, route_weights.T,
        gate_proj, up_proj, expert_down, output_gain.reshape(1, 512),
    )


def solution(mesh):
    placed = (
        P("ep", None), P(), P("ep", "tp"), P("ep", "tp"), P("ep", "tp"), P("ep", "tp"),
        P("tp", None), P("tp", None), P("ep", "tp", None, None), P("ep", "tp"), P("tp"),
        P(None, "ep"), P("ep"), P("ep"), P(), P(), P("ep", None, "tp"), P("ep", None, "tp"),
        P("ep", "tp", None), P("tp"),
    )
    return jax.shard_map(
        shards, mesh=mesh, in_specs=placed, out_specs=P("ep", "tp"), check_vma=False
    )
```

time: 248 us -> 68.7 us (0.28)
  waiting for transfers between devices: 110 us -> 0 us
  Pallas kernels: 0 us -> 67.2 us
  local copies, waits for them, and re-layouts: 33.7 us -> 1.32 us
  starting transfers between devices: 28.6 us -> 0 us
  blocking collectives: 26.9 us -> 0 us
  matrix products: 24 us -> 0 us
  between operations: 13.8 us -> 0.01 us
  other arithmetic: 9.5 us -> 0 us
    all_gather x2 -> x0, waiting for transfers between devices: 82.8 us -> none  [the longest x1 55.6 us: in_one_piece(): lax.all_gather(both, axis, axis=dim, tiled=True)]
    pallas_call x0 -> x1, Pallas kernels: none -> 67.2 us  [shards(): pl.pallas_call(body, out_shape=jax.ShapeDtypeStruct((16, 512), BF16), in_...]
    all_to_all x6 -> x0, starting transfers between devices: 28.6 us -> none  [the longest x2 8.52 us: copy_for_each(): lax.all_to_all(jnp.broadcast_to(shard[None], (devices, *shard.shape)), ax...]
    all_to_all x6 -> x0, waiting for transfers between devices: 27.4 us -> none  [the longest x1 7.67 us: sent_and_summed(): lax.all_to_all(cut_along(shard, dim, devices), axis, 0, 0, tiled=True)]
    all_to_all x2 -> x0, blocking collectives: 26.9 us -> none  [the longest x1 18.6 us: shards(): lax.all_to_all(outgoing, 'ep', split_axis=0, concat_axis=2, tiled=True)]
    dot_general x10 -> x0, matrix products: 24 us -> none  [the longest x4 8.11 us: shards(): jnp.dot(normed, matrix, preferred_element_type=jnp.float32)]
    gather x4 -> x0, local copies, waits for them, and re-layouts: 15.9 us -> none  [the longest x2 15.2 us: shards(): outgoing = padded_in[slot_grid]]
    scatter x1 -> x0, local copies, waits for them, and re-layouts: 8.06 us -> none  [slot_tables(): slot_token = jnp.full((experts * groups * capacity,), token_total, jnp.in...]
  transfers between devices with their start and end apart: 8 -> 0, of which waited for: 8 -> 0; matrix products, arithmetic and copies ran while one was open for 8% -> 0% of each run, Pallas kernels for 0% -> 0%
where the time goes in v1:
time: 68.7 us; the launch traced here: 68.5 us
  Pallas kernels  67.2 us (98%)
  local copies, waits for them, and re-layouts  1.32 us (2%)
    pallas_call x1, Pallas kernels, shards(): pl.pallas_call(body, out_shape=jax.ShapeDtypeStruct((16, 512), BF16), in_...  67.2 us

profile of v1, /device:TPU:1, one launch (start us, length us, event | category | flops | bytes accessed | tf_op | source)
XLA Modules:
  0.0 68.5 jit_solution(18358022382489316984)
XLA Ops:
  0.0 67.2 %step.1 = bf16[16,512]{1,0:T(8,128)(2,1)} custom-call(bf16[16,2048]{1,0:T(8,128)(2,1)} %tok_h.1, f32[1,2048]{1,0:T(1,128)} %bitcast.10, bf16[64,512]{1,0:T(8,128)(2,1)} %wq_h.1, bf16[64,512]{1,0:T(8,128)(2,1)} %wk_h.1, bf16[64,512]{1,0:T(8,128)(2,1)} %wv_h.1, bf16[64,512]{1,0:T(8,128)(2,1)} %wo_h.1, bf16[1,2048]{1,0:T(2,128)(2,1)} %ig_h.1, ...), custom_call_target="tpu_custom_call" | custom-call | tf_op jit(solution)/shard_map/step/pallas_call | solution.py:389
  67.2 1.3 %copy.22 = bf16[16,512]{1,0:T(8,128)(2,1)} copy(bf16[16,512]{1,0:T(8,128)(2,1)} %step.1) | data formatting | bytes 32768

commit v2 on v1

--- a/solution.py
+++ b/solution.py
@@ -11,8 +11,9 @@
 SIG = 1.702
 F32 = jnp.float32
 BF16 = jnp.bfloat16
-N_REMOTE = 96
-N_LOCAL = 48
+N_SEND = 14
+N_RECV = 19
+N_LOCAL = 15
 
 
 def iota(shape, dim):
@@ -53,40 +54,56 @@
     def xdev(xx):
         return {"tp": xx}
 
-    count = [0, 0]
-    sent = []
-
-    def rcopy(src, dst, dev):
-        i = count[0]
-        count[0] += 1
+    sems = [0, 0, 0]
+
+    def ssem():
+        sems[0] += 1
+        return ss.at[sems[0] - 1]
+
+    def rsem():
+        sems[1] += 1
+        return rs.at[sems[1] - 1]
+
+    def lsem():
+        sems[2] += 1
+        return ls.at[sems[2] - 1]
+
+    def rcopy(src, dst, dev, s_sem, r_sem, go=True):
         cp = pltpu.make_async_remote_copy(
-            src_ref=src, dst_ref=dst, send_sem=ss.at[i], recv_sem=rs.at[i],
+            src_ref=src, dst_ref=dst, send_sem=s_sem, recv_sem=r_sem,
             device_id=dev, device_id_type=pl.DeviceIdType.MESH,
         )
-        cp.start()
-        sent.append(cp)
+        if go:
+            cp.start()
         return cp
 
-    def lcopy(src, dst):
-        i = count[1]
-        count[1] += 1
-        cp = pltpu.make_async_copy(src, dst, ls.at[i])
+    ends = []
+
+    def group(like):
+        s_sem, r_sem = ssem(), rsem()
+        whole = rcopy(like, like, partner, s_sem, r_sem, go=False)
+        ends.append(whole)
+        return s_sem, r_sem, whole
+
+    def lcopy(src, dst, sem=None):
+        cp = pltpu.make_async_copy(src, dst, lsem() if sem is None else sem)
         cp.start()
         return cp
 
+    w_sem = lsem()
+    l_w = [
+        lcopy(wq_h, wa.at[0, z, c], w_sem), lcopy(wv_h, wa.at[1, z, c], w_sem),
+        lcopy(wk_h, wb.at[0, y, c], w_sem), lcopy(wo_h, wb.at[1, y, c], w_sem),
+    ]
+    own_rows = pl.ds(pl.multiple_of(t * 512, 512), 512)
+    l_dw = lcopy(dw_h.at[:, own_rows], dt.at[z, y, c])
+    l_g = [lcopy(mg_h, mg), lcopy(eg_h, eg)]
     l_tok = lcopy(tok_h, tok)
     l_mixg = lcopy(mixg_h, mixg)
-    l_w = [
-        lcopy(wq_h, wa.at[0, z, c]), lcopy(wv_h, wa.at[1, z, c]),
-        lcopy(wk_h, wb.at[0, y, c]), lcopy(wo_h, wb.at[1, y, c]),
-    ]
-    l_g = [lcopy(mg_h, mg), lcopy(eg_h, eg)]
     l_small = [
         lcopy(ig_h, ig), lcopy(fg_h, fg), lcopy(stab_h, stab), lcopy(hg_h, hg),
         lcopy(rt_h, rt), lcopy(rw_h, rw), lcopy(og_h, og),
     ]
-    own_rows = pl.ds(pl.multiple_of(t * 512, 512), 512)
-    l_dw = lcopy(dw_h.at[:, own_rows], dt.at[z, y, c])
 
     bar = pltpu.get_barrier_semaphore()
     near = [partner]
@@ -94,23 +111,35 @@
         near += [zdev((z + d) % 4), ydev((y + d) % 4), xdev((t + d) % 4)]
     for dev in near:
         pl.semaphore_signal(bar, inc=1, device_id=dev, device_id_type=pl.DeviceIdType.MESH)
+
+    for cp in l_g:
+        cp.wait()
+    spread = ((iota((64, 128), 1) & 63) == iota((64, 128), 0)).astype(F32)
+    mg128 = jnp.dot(jnp.broadcast_to(mg[...], (8, 64)), spread, precision=lax.Precision.HIGHEST, preferred_element_type=F32)
+    eg128 = jnp.dot(jnp.broadcast_to(eg[...], (8, 64)), spread, precision=lax.Precision.HIGHEST, preferred_element_type=F32)
+    gains[z, y, c] = jnp.where(iota((8, 128), 0) == 0, mg128, eg128)
+    l_dw.wait()
+    pltpu.make_async_copy(wa.at[:, 0:1], wa.at[:, 0:1], w_sem).wait()
     pl.semaphore_wait(bar, len(near))
 
+    s1, r1, d1_in = group(dt.at[0:3, 0, 0])
+    g1s, g1r, g1_in = group(gains.at[0:3, 0, 0])
+    for d in (2, 1, 3):
+        zz, yy = (z + d) % 4, (y + d) % 4
+        rcopy(dt.at[z, y, c, :, 0:256], dt.at[z, y, c, :, 0:256], zdev(zz), s1, r1)
+        rcopy(dt.at[z, y, c, :, 256:512], dt.at[z, y, c, :, 256:512], ydev(yy), s1, r1)
+        rcopy(gains.at[z, y, c], gains.at[z, y, c], zdev(zz), g1s, g1r)
+
+    sw, rp, p_in = group(wa)
     a_in, b_in = {}, {}
     for d in (2, 1, 3):
         zz, yy = (z + d) % 4, (y + d) % 4
-        a_in[d] = [
-            rcopy(wq_h, wa.at[0, z, c], zdev(zz)), rcopy(wv_h, wa.at[1, z, c], zdev(zz)),
-        ]
-        b_in[d] = [
-            rcopy(wk_h, wb.at[0, y, c], ydev(yy)), rcopy(wo_h, wb.at[1, y, c], ydev(yy)),
-        ]
-    p_in = [
-        rcopy(wq_h, wa.at[0, z, c], partner), rcopy(wv_h, wa.at[1, z, c], partner),
-        rcopy(wk_h, wb.at[0, y, c], partner), rcopy(wo_h, wb.at[1, y, c], partner),
-    ]
-    l_mem = [lcopy(mem_h.at[pl.ds(2 * i, 2), 0], mem.at[pl.ds(2 * i, 2)]) for i in range(8)]
-    l_exp = [lcopy(w1_h.at[0], w1), lcopy(w3_h.at[0], w3), lcopy(w2_h.at[0], w2)]
+        a_in[d] = rcopy(wa.at[:, z, c], wa.at[:, z, c], zdev(zz), sw, rsem())
+        b_in[d] = rcopy(wb.at[:, y, c], wb.at[:, y, c], ydev(yy), sw, rsem())
+    rcopy(wa.at[:, z, c], wa.at[:, z, c], partner, sw, rp)
+    rcopy(wb.at[:, y, c], wb.at[:, y, c], partner, sw, rp)
+    sf = ssem()
+    ends.append(rcopy(wa.at[:, 0:3], wa.at[:, 0:3], partner, sf, rp, go=False))
 
     l_tok.wait()
     l_mixg.wait()
@@ -123,27 +152,17 @@
             na[yy, :, zz * 128:(zz + 1) * 128] = normed[:, zz * 512 + yy * 128:zz * 512 + yy * 128 + 128]
     xa[y] = na[y]
     xb[z] = nrm[:, pl.ds(pl.multiple_of(z * 512, 512), 512)]
-    ta_in, tb_in = [], []
-    for d in (2, 1, 3):
-        zz, yy = (z + d) % 4, (y + d) % 4
-        ta_in.append(rcopy(na.at[yy], xa.at[y], ydev(yy)))
-        tb_in.append(rcopy(nrm.at[:, pl.ds(pl.multiple_of(zz * 512, 512), 512)], xb.at[z], zdev(zz)))
-
-    da_in, db_in = [], []
-    for d in (2, 1, 3):
-        zz, yy = (z + d) % 4, (y + d) % 4
-        lo = pl.ds(pl.multiple_of(t * 512, 256), 256)
-        hi = pl.ds(pl.multiple_of(t * 512 + 256, 256), 256)
-        da_in.append(rcopy(dw_h.at[:, lo], dt.at[z, y, c, :, 0:256], zdev(zz)))
-        db_in.append(rcopy(dw_h.at[:, hi], dt.at[z, y, c, :, 256:512], ydev(yy)))
-
-    for cp in l_g:
-        cp.wait()
-    spread = ((iota((64, 128), 1) & 63) == iota((64, 128), 0)).astype(F32)
-    mg128 = jnp.dot(jnp.broadcast_to(mg[...], (8, 64)), spread, precision=lax.Precision.HIGHEST, preferred_element_type=F32)
-    eg128 = jnp.dot(jnp.broadcast_to(eg[...], (8, 64)), spread, precision=lax.Precision.HIGHEST, preferred_element_type=F32)
-    gains[z, y, c] = jnp.where(iota((8, 128), 0) == 0, mg128, eg128)
-    g1_in = [rcopy(gains.at[z, y, c], gains.at[z, y, c], zdev((z + d) % 4)) for d in (2, 1, 3)]
+    st_, rt_, t_in = group(ra.at[0:3])
+    for d in (2, 1, 3):
+        zz, yy = (z + d) % 4, (y + d) % 4
+        rcopy(na.at[yy], xa.at[y], ydev(yy), st_, rt_)
+        rcopy(nrm.at[:, pl.ds(pl.multiple_of(zz * 512, 512), 512)], xb.at[z], zdev(zz), st_, rt_)
+
+    m_sem, e_sem = lsem(), lsem()
+    for i in range(8):
+        lcopy(mem_h.at[pl.ds(2 * i, 2), 0], mem.at[pl.ds(2 * i, 2)], m_sem)
+    for src, dst in ((w1_h, w1), (w3_h, w3), (w2_h, w2)):
+        lcopy(src.at[0], dst, e_sem)
 
     for cp in l_small:
         cp.wait()
@@ -181,54 +200,55 @@
     perm[...] = (c5 == 16 * ((r5 & 127) >> 2) + 4 * (r5 >> 7) + (r5 & 3)).astype(BF16)
     permt[...] = (r5 == 16 * ((c5 & 127) >> 2) + 4 * (c5 >> 7) + (c5 & 3)).astype(BF16)
 
-    f_in = []
-    for n, d in enumerate((1, 3, 2)):
+    d1_in.wait_recv()
+    g1_in.wait_recv()
+    s2, r2, d2_in = group(dt.at[0:3, :, 0])
+    g2s, g2r, g2_in = group(gains.at[0:3, :, 0])
+    for d in (2, 1, 3):
+        zz, yy = (z + d) % 4, (y + d) % 4
+        rcopy(gains.at[:, y, c], gains.at[:, y, c], ydev(yy), g2s, g2r)
+        rcopy(dt.at[:, y, c, :, 0:256], dt.at[:, y, c, :, 0:256], ydev(yy), s2, r2)
+        rcopy(dt.at[z, :, c, :, 256:512], dt.at[z, :, c, :, 256:512], zdev(zz), s2, r2)
+
+    for d in (1, 3, 2):
         zz, yy = (z + 4 - d) % 4, (y + 4 - d) % 4
-        for cp in a_in[d]:
-            cp.wait_recv()
-        f_in.append(rcopy(wa.at[:, zz, c], wa.at[:, zz, c], partner))
-        for cp in b_in[d]:
-            cp.wait_recv()
-        f_in.append(rcopy(wb.at[:, yy, c], wb.at[:, yy, c], partner))
-    for cp in ta_in + tb_in:
-        cp.wait_recv()
-    for cp in l_w:
-        cp.wait()
-    for cp in p_in + f_in:
-        cp.wait_recv()
+        a_in[d].wait_recv()
+        rcopy(wa.at[:, zz, c], wa.at[:, zz, c], partner, sf, rp)
+        b_in[d].wait_recv()
+        rcopy(wb.at[:, yy, c], wb.at[:, yy, c], partner, sf, rp)
+    t_in.wait_recv()
+    p_in.wait_recv()
 
     ax = xa[...].reshape(64, 512)
     bx = xb[...].reshape(64, 512)
     sa[...] = mm(ax, wa[0].reshape(512, 512)).reshape(4, 16, 512)
     sb[...] = mm(bx, wb[0].reshape(512, 512)).reshape(4, 16, 512)
-    pr_in = []
-    for d in (2, 1, 3):
-        zz, yy = (z + d) % 4, (y + d) % 4
-        pr_in.append(rcopy(sa.at[yy], ra.at[y], ydev(yy)))
-        pr_in.append(rcopy(sb.at[zz], rb.at[z], zdev(zz)))
+    sq_, rq_, q_in = group(dt.at[0:3, 0, 0])
+    sv_, rv_, v_in = group(ra.at[0:3])
+    for d in (2, 1, 3):
+        zz, yy = (z + d) % 4, (y + d) % 4
+        rcopy(sa.at[yy], ra.at[y], ydev(yy), sq_, rq_)
+        rcopy(sb.at[zz], rb.at[z], zdev(zz), sq_, rq_)
     sa2[...] = mm(ax, wa[1].reshape(512, 512)).astype(BF16).reshape(4, 16, 512)
     sb2[...] = mm(bx, wb[1].reshape(512, 512)).astype(BF16).reshape(4, 16, 512)
     for d in (2, 1, 3):
         zz, yy = (z + d) % 4, (y + d) % 4
-        pr_in.append(rcopy(sa2.at[yy], ra2.at[y], ydev(yy)))
-        pr_in.append(rcopy(sb2.at[zz], rb2.at[z], zdev(zz)))
+        rcopy(sa2.at[yy], ra2.at[y], ydev(yy), sv_, rv_)
+        rcopy(sb2.at[zz], rb2.at[z], zdev(zz), sv_, rv_)
     ra[y] = sa[y]
     rb[z] = sb[z]
     ra2[y] = sa2[y]
     rb2[z] = sb2[z]
 
-    l_dw.wait()
-    for cp in da_in + db_in + g1_in:
-        cp.wait_recv()
-    d2_in = []
-    for d in (2, 1, 3):
-        zz, yy = (z + d) % 4, (y + d) % 4
-        d2_in.append(rcopy(gains.at[:, y, c], gains.at[:, y, c], ydev(yy)))
-        d2_in.append(rcopy(dt.at[:, y, c, :, 0:256], dt.at[:, y, c, :, 0:256], ydev(yy)))
-        d2_in.append(rcopy(dt.at[z, :, c, :, 256:512], dt.at[z, :, c, :, 256:512], zdev(zz)))
-
-    for cp in pr_in:
-        cp.wait_recv()
+    d2_in.wait_recv()
+    g2_in.wait_recv()
+    s3, r3, d3_in = group(dt.at[:, :, 0])
+    g3s, g3r, g3_in = group(gains.at[:, :, 0])
+    rcopy(dt.at[:, :, c], dt.at[:, :, c], partner, s3, r3)
+    rcopy(gains.at[:, :, c], gains.at[:, :, c], partner, g3s, g3r)
+
+    q_in.wait_recv()
+    v_in.wait_recv()
     q = jnp.sum(ra[...], axis=0).astype(BF16).astype(F32) * (512.0 ** -0.5)
     key = jnp.sum(rb[...], axis=0).astype(BF16).astype(F32)
     val = jnp.sum(ra2[...].astype(F32), axis=0)
@@ -236,40 +256,35 @@
     qpad[0:16, :] = q
     qpad[16:128, :] = jnp.zeros((112, 512), F32)
     qt[...] = jnp.transpose(qpad[...])
-    for cp in l_mem:
-        cp.wait()
+    pltpu.make_async_copy(mem, mem, m_sem).wait()
     for n in range(16):
         qcol = qt[:, n:n + 1]
         read[n:n + 1, :] = jnp.sum(qcol * mem[n], axis=0, keepdims=True)
 
-    for cp in d2_in:
-        cp.wait_recv()
-    d3_in = [
-        rcopy(dt.at[:, :, c], dt.at[:, :, c], partner),
-        rcopy(gains.at[:, :, c], gains.at[:, :, c], partner),
-    ]
     score = jnp.sum(q * key, axis=-1, keepdims=True) * within
     rd = score * val + carried * read[...]
     mean = jnp.mean(rd, axis=-1, keepdims=True)
     cen = rd - mean
     var = jnp.mean(cen * cen, axis=-1, keepdims=True)
     gated = (cen * lax.rsqrt(var + EPS) * hg[...] * sigmoid(og_pre)).astype(BF16)
-    for cp in d3_in:
-        cp.wait_recv()
-
-    part = lax.dot_general(
-        gated, dt[...].reshape(2048, 512), (((1,), (1,)), ((), ())), preferred_element_type=F32
-    )
-    mx[t] = part.astype(BF16)
-    m_in = [rcopy(mx.at[t], mx.at[t], xdev((t + d) % 4)) for d in (2, 1, 3)]
+    d3_in.wait_recv()
+    g3_in.wait_recv()
+    sm, rm, m_in = group(mx.at[0:3])
+    for k in range(4):
+        cols = pl.ds(k * 512, 512)
+        part = lax.dot_general(
+            gated, dt[k].reshape(512, 512), (((1,), (1,)), ((), ())), preferred_element_type=F32
+        )
+        mx[t, :, cols] = part.astype(BF16)
+        for d in (2, 1, 3):
+            rcopy(mx.at[t, :, cols], mx.at[t, :, cols], xdev((t + d) % 4), sm, rm)
     low = iota((1, 128), 1) < 64
     for zz in range(4):
         for yy in range(4):
             at = zz * 512 + yy * 128
             g0, g1 = gains[zz, yy, 0], gains[zz, yy, 1]
             gfull[:, at:at + 128] = jnp.where(low, g0, g1)
-    for cp in m_in:
-        cp.wait_recv()
+    m_in.wait_recv()
     mixed = jnp.sum(mx[...].astype(F32), axis=0)
     xf = tok[...].astype(F32)
     mixed_gain = gfull[0:1, :]
@@ -313,8 +328,7 @@
         )
 
     ex1 = exchange(do, di, 0)
-    for cp in l_exp:
-        cp.wait()
+    pltpu.make_async_copy(mem.at[0:6], mem.at[0:6], e_sem).wait()
     ex1.wait_recv()
     yst[...] = mm(perm[...], di[...]).astype(BF16)
     gate = jnp.zeros((128, 512), F32)
@@ -326,15 +340,14 @@
     gate = jnp.minimum(gate, LIMIT)
     up = jnp.clip(up, -LIMIT, LIMIT)
     act[...] = ((up + 1.0) * gate * sigmoid(SIG * gate)).astype(BF16)
-    x_in = []
+    sxs, rxs, x_in = group(rx)
     for d in (2, 1, 3):
         tt = (t + d) % 4
         blk = mm(act[...], w2[:, pl.ds(pl.multiple_of(tt * 512, 512), 512)])
         sx[d - 1] = blk.astype(BF16)
-        x_in.append(rcopy(sx.at[d - 1], rx.at[d - 1], xdev(tt)))
+        rcopy(sx.at[d - 1], rx.at[d - 1], xdev(tt), sxs, rxs)
     own_x[...] = mm(act[...], w2[:, own_rows])
-    for cp in x_in:
-        cp.wait_recv()
+    x_in.wait_recv()
     red = own_x[...] + jnp.sum(rx[...].astype(F32), axis=0)
     redb = red.astype(BF16)
     for k in range(4):
@@ -345,16 +358,18 @@
     comb4 = mm(ohw_hi[...], zi[...]) + mm(ohw_lo[...], zi[...])
     comb = jnp.concatenate([comb4[k * 16:(k + 1) * 16, :] for k in range(4)], axis=1)
     sq[t] = jnp.broadcast_to(jnp.sum(comb * comb, axis=-1, keepdims=True), (16, 128))
-    s_in = [rcopy(sq.at[t], sq.at[t], xdev((t + d) % 4)) for d in (2, 1, 3)]
-    for cp in s_in:
-        cp.wait_recv()
+    sqs, sqr, s_in = group(sq.at[0:3])
+    for d in (2, 1, 3):
+        rcopy(sq.at[t], sq.at[t], xdev((t + d) % 4), sqs, sqr)
+    s_in.wait_recv()
     total = jnp.sum(sq[...], axis=0)[:, 0:1]
     mine = resid[:, own_rows].astype(F32)
     out[...] = (mine + comb * lax.rsqrt(total * (1.0 / 2048.0) + EPS) * og[...]).astype(BF16)
-    for cp in sent:
+    for cp in ends:
         cp.wait_send()
     ex1.wait_send()
     ex2.wait_send()
+    assert sems == [N_SEND, N_RECV, N_LOCAL], sems
 
 
 def shards(
@@ -382,7 +397,7 @@
         V((512, 512), BF16), V((512, 512), BF16), V((512, 512), BF16), V((128, 512), BF16),
         V((3, 128, 512), BF16), V((3, 128, 512), BF16), V((128, 512), F32), V((512, 128), BF16),
         V((512, 128), BF16), V((512, 128), BF16), V((4, 16, 128), F32),
-        pltpu.SemaphoreType.DMA((N_REMOTE,)), pltpu.SemaphoreType.DMA((N_REMOTE,)),
+        pltpu.SemaphoreType.DMA((N_SEND,)), pltpu.SemaphoreType.DMA((N_RECV,)),
         pltpu.SemaphoreType.DMA((N_LOCAL,)),
         pltpu.SemaphoreType.DMA((2,)), pltpu.SemaphoreType.DMA((2,)),
     ]

time: 68.7 us -> 62 us (0.902)
  Pallas kernels: 67.2 us -> 60.5 us
    pallas_call x1, Pallas kernels: 67.2 us -> 60.5 us  [shards(): pl.pallas_call(body, out_shape=jax.ShapeDtypeStruct((16, 512), BF16), in_...]
where the time goes in v2:
time: 62 us; the launch traced here: 61.8 us
  Pallas kernels  60.5 us (98%)
  local copies, waits for them, and re-layouts  1.32 us (2%)
    pallas_call x1, Pallas kernels, shards(): pl.pallas_call(body, out_shape=jax.ShapeDtypeStruct((16, 512), BF16), in_...  60.5 us
    unnamed x1, local copies, waits for them, and re-layouts  1.32 us

profile of v2, /device:TPU:1, one launch (start us, length us, event | category | flops | bytes accessed | tf_op | source)
XLA Modules:
  0.0 61.8 jit_solution(14168009555995172063)
XLA Ops:
  0.0 60.5 %step.1 = bf16[16,512]{1,0:T(8,128)(2,1)} custom-call(bf16[16,2048]{1,0:T(8,128)(2,1)} %tok_h.1, f32[1,2048]{1,0:T(1,128)} %bitcast.10, bf16[64,512]{1,0:T(8,128)(2,1)} %wq_h.1, bf16[64,512]{1,0:T(8,128)(2,1)} %wk_h.1, bf16[64,512]{1,0:T(8,128)(2,1)} %wv_h.1, bf16[64,512]{1,0:T(8,128)(2,1)} %wo_h.1, bf16[1,2048]{1,0:T(2,128)(2,1)} %ig_h.1, ...), custom_call_target="tpu_custom_call" | custom-call | tf_op jit(solution)/shard_map/step/pallas_call | solution.py:404
  60.5 1.3 %copy.22 = bf16[16,512]{1,0:T(8,128)(2,1)} copy(bf16[16,512]{1,0:T(8,128)(2,1)} %step.1) | data formatting | bytes 32768

commit v3 on v2

--- a/solution.py
+++ b/solution.py
@@ -11,8 +11,8 @@
 SIG = 1.702
 F32 = jnp.float32
 BF16 = jnp.bfloat16
-N_SEND = 14
-N_RECV = 19
+N_SEND = 15
+N_RECV = 20
 N_LOCAL = 15
 
 
@@ -33,9 +33,9 @@
     mg_h, eg_h, rt_h, rw_h, w1_h, w3_h, w2_h, og_h,
     out,
     tok, mixg, wa, wb, ig, fg, mem, stab, hg, dt, mg, eg, gains, rt, rw, w1, w3, w2, og,
-    nrm, na, xa, xb, sa, sb, ra, rb, sa2, sb2, ra2, rb2, qpad, qt, read,
+    nrm, na, xa, xb, sa, sb, ra, rb, qpad, qt, read,
     mx, gfull, resid, xst, oh_s, ohw_hi, ohw_lo, perm, permt,
-    do, di, yst, act, sx, rx, own_x, rst, zo, zi, sq,
+    do, di, yst, act, sx, rx, own_x, rst, zo, zi, bst, zbo, zbi, cbs, cbr, sq,
     ss, rs, ls, a2a_s, a2a_r,
 ):
     ep = lax.axis_index("ep")
@@ -92,8 +92,8 @@
 
     w_sem = lsem()
     l_w = [
-        lcopy(wq_h, wa.at[0, z, c], w_sem), lcopy(wv_h, wa.at[1, z, c], w_sem),
-        lcopy(wk_h, wb.at[0, y, c], w_sem), lcopy(wo_h, wb.at[1, y, c], w_sem),
+        lcopy(wv_h, wa.at[0, z, c], w_sem), lcopy(wo_h, wa.at[1, z, c], w_sem),
+        lcopy(wq_h, wb.at[0, y, c], w_sem), lcopy(wk_h, wb.at[1, y, c], w_sem),
     ]
     own_rows = pl.ds(pl.multiple_of(t * 512, 512), 512)
     l_dw = lcopy(dw_h.at[:, own_rows], dt.at[z, y, c])
@@ -221,24 +221,22 @@
 
     ax = xa[...].reshape(64, 512)
     bx = xb[...].reshape(64, 512)
-    sa[...] = mm(ax, wa[0].reshape(512, 512)).reshape(4, 16, 512)
-    sb[...] = mm(bx, wb[0].reshape(512, 512)).reshape(4, 16, 512)
     sq_, rq_, q_in = group(dt.at[0:3, 0, 0])
     sv_, rv_, v_in = group(ra.at[0:3])
-    for d in (2, 1, 3):
-        zz, yy = (z + d) % 4, (y + d) % 4
-        rcopy(sa.at[yy], ra.at[y], ydev(yy), sq_, rq_)
-        rcopy(sb.at[zz], rb.at[z], zdev(zz), sq_, rq_)
-    sa2[...] = mm(ax, wa[1].reshape(512, 512)).astype(BF16).reshape(4, 16, 512)
-    sb2[...] = mm(bx, wb[1].reshape(512, 512)).astype(BF16).reshape(4, 16, 512)
-    for d in (2, 1, 3):
-        zz, yy = (z + d) % 4, (y + d) % 4
-        rcopy(sa2.at[yy], ra2.at[y], ydev(yy), sv_, rv_)
-        rcopy(sb2.at[zz], rb2.at[z], zdev(zz), sv_, rv_)
+    for k in range(2):
+        cols = pl.ds(k * 512, 512)
+        sb[:, :, cols] = mm(bx, wb[k].reshape(512, 512)).reshape(4, 16, 512)
+        for d in (2, 1, 3):
+            zz = (z + d) % 4
+            rcopy(sb.at[zz, :, cols], rb.at[z, :, cols], zdev(zz), sq_, rq_)
+    for k in range(2):
+        cols = pl.ds(k * 512, 512)
+        sa[:, :, cols] = mm(ax, wa[k].reshape(512, 512)).astype(BF16).reshape(4, 16, 512)
+        for d in (2, 1, 3):
+            yy = (y + d) % 4
+            rcopy(sa.at[yy, :, cols], ra.at[y, :, cols], ydev(yy), sv_, rv_)
     ra[y] = sa[y]
     rb[z] = sb[z]
-    ra2[y] = sa2[y]
-    rb2[z] = sb2[z]
 
     d2_in.wait_recv()
     g2_in.wait_recv()
@@ -249,10 +247,12 @@
 
     q_in.wait_recv()
     v_in.wait_recv()
-    q = jnp.sum(ra[...], axis=0).astype(BF16).astype(F32) * (512.0 ** -0.5)
-    key = jnp.sum(rb[...], axis=0).astype(BF16).astype(F32)
-    val = jnp.sum(ra2[...].astype(F32), axis=0)
-    og_pre = jnp.sum(rb2[...].astype(F32), axis=0)
+    qk = jnp.sum(rb[...], axis=0).astype(BF16).astype(F32)
+    q = qk[:, 0:512] * (512.0 ** -0.5)
+    key = qk[:, 512:]
+    vo = jnp.sum(ra[...].astype(F32), axis=0)
+    val = vo[:, 0:512]
+    og_pre = vo[:, 512:]
     qpad[0:16, :] = q
     qpad[16:128, :] = jnp.zeros((112, 512), F32)
     qt[...] = jnp.transpose(qpad[...])
@@ -340,23 +340,35 @@
     gate = jnp.minimum(gate, LIMIT)
     up = jnp.clip(up, -LIMIT, LIMIT)
     act[...] = ((up + 1.0) * gate * sigmoid(SIG * gate)).astype(BF16)
+    for k in range(4):
+        blk = mm(act[...], w2[:, k * 512 + 256:(k + 1) * 512])
+        bst[k * 128:(k + 1) * 128, :] = blk.astype(BF16)
+    zbo[...] = mm(permt[...], bst[...]).astype(BF16)
+    ex2 = exchange(zbo, zbi, 1)
     sxs, rxs, x_in = group(rx)
     for d in (2, 1, 3):
         tt = (t + d) % 4
-        blk = mm(act[...], w2[:, pl.ds(pl.multiple_of(tt * 512, 512), 512)])
+        blk = mm(act[...], w2[:, pl.ds(pl.multiple_of(tt * 512, 512), 256)])
         sx[d - 1] = blk.astype(BF16)
         rcopy(sx.at[d - 1], rx.at[d - 1], xdev(tt), sxs, rxs)
-    own_x[...] = mm(act[...], w2[:, own_rows])
+    own_x[...] = mm(act[...], w2[:, pl.ds(pl.multiple_of(t * 512, 512), 256)])
     x_in.wait_recv()
-    red = own_x[...] + jnp.sum(rx[...].astype(F32), axis=0)
-    redb = red.astype(BF16)
-    for k in range(4):
-        rst[k * 128:(k + 1) * 128, :] = redb[:, k * 128:(k + 1) * 128]
-    zo[...] = mm(permt[...], rst[...]).astype(BF16)
-    ex2 = exchange(zo, zi, 1)
+    red = (own_x[...] + jnp.sum(rx[...].astype(F32), axis=0)).astype(BF16)
+    for k in range(2):
+        rst[k * 128:(k + 1) * 128, :] = red[:, k * 128:(k + 1) * 128]
+    zo[...] = mm(permt[:, 0:256], rst[...]).astype(BF16)
+    ex3 = exchange(zo, zi, 2)
     ex2.wait_recv()
-    comb4 = mm(ohw_hi[...], zi[...]) + mm(ohw_lo[...], zi[...])
-    comb = jnp.concatenate([comb4[k * 16:(k + 1) * 16, :] for k in range(4)], axis=1)
+    cbs[...] = (mm(ohw_hi[...], zbi[...]) + mm(ohw_lo[...], zbi[...])).reshape(4, 16, 256)
+    cs_, cr_, c_in = group(cbr)
+    for d in (2, 1, 3):
+        tt = (t + d) % 4
+        rcopy(cbs.at[tt], cbr.at[d - 1], xdev(tt), cs_, cr_)
+    ex3.wait_recv()
+    half4 = mm(ohw_hi[0:32, :], zi[...]) + mm(ohw_lo[0:32, :], zi[...])
+    c_in.wait_recv()
+    beta = cbs[t] + jnp.sum(cbr[...], axis=0)
+    comb = jnp.concatenate([half4[0:16, :], half4[16:32, :], beta], axis=1)
     sq[t] = jnp.broadcast_to(jnp.sum(comb * comb, axis=-1, keepdims=True), (16, 128))
     sqs, sqr, s_in = group(sq.at[0:3])
     for d in (2, 1, 3):
@@ -369,6 +381,7 @@
         cp.wait_send()
     ex1.wait_send()
     ex2.wait_send()
+    ex3.wait_send()
     assert sems == [N_SEND, N_RECV, N_LOCAL], sems
 
 
@@ -388,22 +401,23 @@
         V((4, 512), jnp.int32), V((4, 512), F32),
         V((2048, 512), BF16), V((2048, 512), BF16), V((512, 2048), BF16), V((1, 512), F32),
         V((16, 2048), BF16), V((4, 16, 512), BF16), V((4, 16, 512), BF16), V((4, 16, 512), BF16),
-        V((4, 16, 512), F32), V((4, 16, 512), F32), V((4, 16, 512), F32), V((4, 16, 512), F32),
-        V((4, 16, 512), BF16), V((4, 16, 512), BF16), V((4, 16, 512), BF16), V((4, 16, 512), BF16),
+        V((4, 16, 1024), BF16), V((4, 16, 1024), F32), V((4, 16, 1024), BF16), V((4, 16, 1024), F32),
         V((128, 512), F32), V((512, 128), F32), V((16, 512), F32),
         V((4, 16, 2048), BF16), V((8, 2048), F32), V((16, 2048), BF16), V((64, 512), BF16),
         V((512, 64), BF16), V((64, 512), BF16), V((64, 512), BF16),
         V((512, 512), BF16), V((512, 512), BF16),
         V((512, 512), BF16), V((512, 512), BF16), V((512, 512), BF16), V((128, 512), BF16),
-        V((3, 128, 512), BF16), V((3, 128, 512), BF16), V((128, 512), F32), V((512, 128), BF16),
-        V((512, 128), BF16), V((512, 128), BF16), V((4, 16, 128), F32),
+        V((3, 128, 256), BF16), V((3, 128, 256), BF16), V((128, 256), F32), V((256, 128), BF16),
+        V((512, 128), BF16), V((512, 128), BF16),
+        V((512, 256), BF16), V((512, 256), BF16), V((512, 256), BF16),
+        V((4, 16, 256), F32), V((3, 16, 256), F32), V((4, 16, 128), F32),
         pltpu.SemaphoreType.DMA((N_SEND,)), pltpu.SemaphoreType.DMA((N_RECV,)),
         pltpu.SemaphoreType.DMA((N_LOCAL,)),
-        pltpu.SemaphoreType.DMA((2,)), pltpu.SemaphoreType.DMA((2,)),
+        pltpu.SemaphoreType.DMA((3,)), pltpu.SemaphoreType.DMA((3,)),
     ]
     return pl.pallas_call(
         body,
-        out_shape=jax.ShapeDtypeStruct((16, 512), BF16),
+        out_shape=pltpu.VMEM((16, 512), BF16),
         in_specs=[pl.BlockSpec(memory_space=pl.ANY)] * 20,
         out_specs=pl.BlockSpec(memory_space=pltpu.VMEM),
         scratch_shapes=scratch,

time: 62 us -> 59.6 us (0.961)
  Pallas kernels: 60.5 us -> 58.8 us
  local copies, waits for them, and re-layouts: 1.32 us -> 0.61 us
    pallas_call x1, Pallas kernels: 60.5 us -> 58.8 us  [shards(): pl.pallas_call(body, out_shape=pltpu.VMEM((16, 512), BF16), in_specs=[pl....]
    unnamed x1, local copies, waits for them, and re-layouts: 1.32 us -> 0.61 us
where the time goes in v3:
time: 59.6 us; the launch traced here: 59.4 us
  Pallas kernels  58.8 us (99%)
  local copies, waits for them, and re-layouts  0.61 us (1%)
    pallas_call x1, Pallas kernels, shards(): pl.pallas_call(body, out_shape=pltpu.VMEM((16, 512), BF16), in_specs=[pl....  58.8 us

profile of v3, /device:TPU:1, one launch (start us, length us, event | category | flops | bytes accessed | tf_op | source)
XLA Modules:
  0.0 59.4 jit_solution(9774835927224697352)
XLA Ops:
  0.0 58.8 %step.1 = bf16[16,512]{1,0:T(8,128)(2,1)S(1)} custom-call(bf16[16,2048]{1,0:T(8,128)(2,1)} %tok_h.1, f32[1,2048]{1,0:T(1,128)} %bitcast.10, bf16[64,512]{1,0:T(8,128)(2,1)} %wq_h.1, bf16[64,512]{1,0:T(8,128)(2,1)} %wk_h.1, bf16[64,512]{1,0:T(8,128)(2,1)} %wv_h.1, bf16[64,512]{1,0:T(8,128)(2,1)} %wo_h.1, bf16[1,2048]{1,0:T(2,128)(2,1)} %ig_h.1, ...), custom_call_target="tpu_custom_call" | custom-call | tf_op jit(solution)/shard_map/step/pallas_call | solution.py:418
  58.8 0.6 %copy.22 = bf16[16,512]{1,0:T(8,128)(2,1)} copy(bf16[16,512]{1,0:T(8,128)(2,1)S(1)} %step.1) | data formatting | bytes 32768

commit v4 on v3

--- a/solution.py
+++ b/solution.py
@@ -35,7 +35,7 @@
     tok, mixg, wa, wb, ig, fg, mem, stab, hg, dt, mg, eg, gains, rt, rw, w1, w3, w2, og,
     nrm, na, xa, xb, sa, sb, ra, rb, qpad, qt, read,
     mx, gfull, resid, xst, oh_s, ohw_hi, ohw_lo, perm, permt,
-    do, di, yst, act, sx, rx, own_x, rst, zo, zi, bst, zbo, zbi, cbs, cbr, sq,
+    do, di, yst, act, sx, rx, own_x, rst, zo, zi, bst, zbo, zbi, cbs, cb, sq,
     ss, rs, ls, a2a_s, a2a_r,
 ):
     ep = lax.axis_index("ep")
@@ -340,18 +340,18 @@
     gate = jnp.minimum(gate, LIMIT)
     up = jnp.clip(up, -LIMIT, LIMIT)
     act[...] = ((up + 1.0) * gate * sigmoid(SIG * gate)).astype(BF16)
+    sxs, rxs, x_in = group(rx)
+    for d in (2, 1, 3):
+        tt = (t + d) % 4
+        blk = mm(act[...], w2[:, pl.ds(pl.multiple_of(tt * 512, 512), 256)])
+        sx[d - 1] = blk.astype(BF16)
+        rcopy(sx.at[d - 1], rx.at[d - 1], xdev(tt), sxs, rxs)
+    own_x[...] = mm(act[...], w2[:, pl.ds(pl.multiple_of(t * 512, 512), 256)])
     for k in range(4):
         blk = mm(act[...], w2[:, k * 512 + 256:(k + 1) * 512])
         bst[k * 128:(k + 1) * 128, :] = blk.astype(BF16)
     zbo[...] = mm(permt[...], bst[...]).astype(BF16)
     ex2 = exchange(zbo, zbi, 1)
-    sxs, rxs, x_in = group(rx)
-    for d in (2, 1, 3):
-        tt = (t + d) % 4
-        blk = mm(act[...], w2[:, pl.ds(pl.multiple_of(tt * 512, 512), 256)])
-        sx[d - 1] = blk.astype(BF16)
-        rcopy(sx.at[d - 1], rx.at[d - 1], xdev(tt), sxs, rxs)
-    own_x[...] = mm(act[...], w2[:, pl.ds(pl.multiple_of(t * 512, 512), 256)])
     x_in.wait_recv()
     red = (own_x[...] + jnp.sum(rx[...].astype(F32), axis=0)).astype(BF16)
     for k in range(2):
@@ -359,22 +359,24 @@
     zo[...] = mm(permt[:, 0:256], rst[...]).astype(BF16)
     ex3 = exchange(zo, zi, 2)
     ex2.wait_recv()
-    cbs[...] = (mm(ohw_hi[...], zbi[...]) + mm(ohw_lo[...], zbi[...])).reshape(4, 16, 256)
-    cs_, cr_, c_in = group(cbr)
-    for d in (2, 1, 3):
-        tt = (t + d) % 4
-        rcopy(cbs.at[tt], cbr.at[d - 1], xdev(tt), cs_, cr_)
+    cb[t] = (mm(ohw_hi[...], zbi[...]) + mm(ohw_lo[...], zbi[...])).astype(BF16).reshape(4, 16, 256)
+    cs_, cr_, c_in = group(cb.at[0:3])
+    for d in (2, 1, 3):
+        rcopy(cb.at[t], cb.at[t], xdev((t + d) % 4), cs_, cr_)
     ex3.wait_recv()
     half4 = mm(ohw_hi[0:32, :], zi[...]) + mm(ohw_lo[0:32, :], zi[...])
+    alpha = jnp.concatenate([half4[0:16, :], half4[16:32, :]], axis=1)
+    sq[t] = jnp.broadcast_to(jnp.sum(alpha * alpha, axis=-1, keepdims=True), (16, 128))
+    sqs, sqr, s_in = group(sq.at[0:3])
+    for d in (2, 1, 3):
+        rcopy(sq.at[t], sq.at[t], xdev((t + d) % 4), sqs, sqr)
     c_in.wait_recv()
-    beta = cbs[t] + jnp.sum(cbr[...], axis=0)
-    comb = jnp.concatenate([half4[0:16, :], half4[16:32, :], beta], axis=1)
-    sq[t] = jnp.broadcast_to(jnp.sum(comb * comb, axis=-1, keepdims=True), (16, 128))
-    sqs, sqr, s_in = group(sq.at[0:3])
-    for d in (2, 1, 3):
-        rcopy(sq.at[t], sq.at[t], xdev((t + d) % 4), sqs, sqr)
+    whole_b = jnp.sum(cb[...].astype(F32), axis=0)
+    cbs[...] = whole_b
+    squares_b = jnp.sum(jnp.sum(whole_b * whole_b, axis=0), axis=-1, keepdims=True)
+    comb = jnp.concatenate([alpha, cbs[t]], axis=1)
     s_in.wait_recv()
-    total = jnp.sum(sq[...], axis=0)[:, 0:1]
+    total = jnp.sum(sq[...], axis=0)[:, 0:1] + squares_b
     mine = resid[:, own_rows].astype(F32)
     out[...] = (mine + comb * lax.rsqrt(total * (1.0 / 2048.0) + EPS) * og[...]).astype(BF16)
     for cp in ends:
@@ -410,7 +412,7 @@
         V((3, 128, 256), BF16), V((3, 128, 256), BF16), V((128, 256), F32), V((256, 128), BF16),
         V((512, 128), BF16), V((512, 128), BF16),
         V((512, 256), BF16), V((512, 256), BF16), V((512, 256), BF16),
-        V((4, 16, 256), F32), V((3, 16, 256), F32), V((4, 16, 128), F32),
+        V((4, 16, 256), F32), V((4, 4, 16, 256), BF16), V((4, 16, 128), F32),
         pltpu.SemaphoreType.DMA((N_SEND,)), pltpu.SemaphoreType.DMA((N_RECV,)),
         pltpu.SemaphoreType.DMA((N_LOCAL,)),
         pltpu.SemaphoreType.DMA((3,)), pltpu.SemaphoreType.DMA((3,)),

time: 59.6 us -> 58.2 us (0.977)
  Pallas kernels: 58.8 us -> 57.4 us
    pallas_call x1, Pallas kernels: 58.8 us -> 57.4 us  [shards(): pl.pallas_call(body, out_shape=pltpu.VMEM((16, 512), BF16), in_specs=[pl....]
where the time goes in v4:
time: 58.2 us; the launch traced here: 58 us
  Pallas kernels  57.4 us (99%)
  local copies, waits for them, and re-layouts  0.61 us (1%)
    pallas_call x1, Pallas kernels, shards(): pl.pallas_call(body, out_shape=pltpu.VMEM((16, 512), BF16), in_specs=[pl....  57.4 us

profile of v4, /device:TPU:1, one launch (start us, length us, event | category | flops | bytes accessed | tf_op | source)
XLA Modules:
  0.0 58.0 jit_solution(3831131260396461091)
XLA Ops:
  0.0 57.4 %step.1 = bf16[16,512]{1,0:T(8,128)(2,1)S(1)} custom-call(bf16[16,2048]{1,0:T(8,128)(2,1)} %tok_h.1, f32[1,2048]{1,0:T(1,128)} %bitcast.10, bf16[64,512]{1,0:T(8,128)(2,1)} %wq_h.1, bf16[64,512]{1,0:T(8,128)(2,1)} %wk_h.1, bf16[64,512]{1,0:T(8,128)(2,1)} %wv_h.1, bf16[64,512]{1,0:T(8,128)(2,1)} %wo_h.1, bf16[1,2048]{1,0:T(2,128)(2,1)} %ig_h.1, ...), custom_call_target="tpu_custom_call" | custom-call | tf_op jit(solution)/shard_map/step/pallas_call | solution.py:420
  57.4 0.6 %copy.22 = bf16[16,512]{1,0:T(8,128)(2,1)} copy(bf16[16,512]{1,0:T(8,128)(2,1)S(1)} %step.1) | data formatting | bytes 32768
